TPU v7x, 256 devices: a whole 4x4x8 slice. The times are simulated.
256 devices in a mesh: ep: 64 (over z, x, core), tp: 4 (over y).
Axes of the slice: x: 4, y: 4, z: 8, core: 2. Of those that a mesh axis runs over, the one named last changes fastest.
Arguments:
- tokens: bfloat16 [65536, 2048], P(('ep', 'tp')), may hold values from -6 to 6
- norm_gain: bfloat16 [2048], replicated, may hold values from 0.099609375 to 1.8984375
- expert_ids: int32 [65536, 2], P(('ep', 'tp')), may hold values from 0 to 63, all different within a row; in each aligned block of 256 rows (0 to 255, 256 to 511, ...) at most 16 rows name the same one
- group_weight: float32 [65536], P(('ep', 'tp')), may hold values from 0.25 to 1
- expert_logit: float32 [65536, 2], P(('ep', 'tp')), may hold values from -4 to 4
- w_gate: bfloat16 [64, 2048, 1024], P('ep', None, 'tp'), may hold values from -0.125 to 0.125
- w_up: bfloat16 [64, 2048, 1024], P('ep', None, 'tp'), may hold values from -0.125 to 0.125
- w_down: bfloat16 [64, 1024, 2048], P('ep', 'tp')
- final_gain: bfloat16 [2048], P('tp'), may hold values from 0.099609375 to 1.8984375
Outputs:
- normed_out: bfloat16 [65536, 2048], P('ep', 'tp')
Inputs may be any that keep to these rules, and one draw needn't show every extreme that they name: `expert_ids`: the 2 experts of a token differ. Among the rows of one device (aligned blocks of 256 tokens) no expert is named more than 16 times, a bound that some block reaches.
All inputs are finite; a program needn't handle non-finite values.
Results may differ from a plain program's by a relative error of at most 0.0058.
Values may be sent and summed in bfloat16 or wider, within the bound.
A program may use at most 128 MiB of HBM per device.

v0:
```python
import jax
import jax.numpy as jnp
from jax import lax
from jax.sharding import PartitionSpec as P

D = 2048


EPS = 1e-06


def sent_together(arrays, axis, dim, along):
    both = jnp.concatenate(arrays, axis=along)
    result, at, finished = (lax.all_gather(both, axis, axis=dim, tiled=True), 0, [])
    for a in arrays:
        finished.append(lax.slice_in_dim(result, at, at + a.shape[along], axis=along))
        at += a.shape[along]
    return tuple(finished)


def sent_to_all(x, axis):
    peers = lax.axis_size(axis)
    return lax.all_to_all(jnp.broadcast_to(x[None], (peers, *x.shape)), axis, 0, 0, tiled=True)


def of_everyone(x, axis):
    return sent_to_all(x, axis).sum(axis=0)


def local(
    tokens, norm_gain, expert_ids, group_weight, expert_logit, w_gate, w_up, w_down, final_gain
):
    tok_dev, width = tokens.shape
    per_token = expert_ids.shape[1]
    exp_dev = w_gate.shape[0]
    experts = exp_dev * lax.axis_size("ep")
    capacity = 2 * tok_dev * per_token // experts
    assigned = tok_dev * per_token
    tokens_f = tokens.astype(jnp.float32)
    inverse_in = lax.rsqrt(jnp.mean(tokens_f * tokens_f, axis=-1, keepdims=True) + EPS)
    normed_in = (tokens_f * inverse_in * norm_gain.astype(jnp.float32)).astype(jnp.bfloat16)
    flat_ids = expert_ids.reshape(assigned)
    onehot = (flat_ids[:, None] == jnp.arange(experts, dtype=jnp.int32)[None, :]).astype(jnp.int32)
    before = jnp.cumsum(onehot, axis=0) - onehot
    slot_rank = jnp.sum(before * onehot, axis=1)
    position = slot_rank * experts + flat_ids
    owner_row = (
        jnp.zeros((capacity * experts,), jnp.int32)
        .at[position]
        .set(jnp.arange(assigned, dtype=jnp.int32) // per_token + 1)
    )
    source = normed_in[jnp.maximum(owner_row - 1, 0)]
    outgoing = jnp.where((owner_row > 0)[:, None], source, jnp.zeros_like(source)).reshape(
        capacity, experts, width
    )
    down_whole = lax.all_gather(w_down, "tp", axis=1, tiled=True)
    gate_whole, up_whole = sent_together((w_gate, w_up), "tp", 2, 0)
    incoming = lax.all_to_all(outgoing, "ep", split_axis=1, concat_axis=1, tiled=True)
    item_count = incoming.shape[0]
    senders = incoming.shape[1] // exp_dev
    arranged = incoming.reshape(item_count, senders, exp_dev, width)
    routed = arranged[:, :, 0, :].reshape(item_count * senders, width)
    gate_full = jnp.dot(routed, gate_whole[0], preferred_element_type=jnp.float32)
    up_full = jnp.dot(routed, up_whole[0], preferred_element_type=jnp.float32)
    hidden = (jax.nn.silu(gate_full) * up_full).astype(jnp.bfloat16)
    product = jnp.dot(hidden, down_whole[0], preferred_element_type=jnp.float32).astype(
        jnp.bfloat16
    )
    results = [product.reshape(item_count, senders, width)]
    answer = jnp.stack(results, axis=2).reshape(item_count, senders * exp_dev, width)
    arrived = lax.all_to_all(answer, "ep", split_axis=1, concat_axis=1, tiled=True)
    picked = arrived.reshape(capacity * experts, width)[position].reshape(tok_dev, per_token, width)
    expert_share = jnp.exp(expert_logit)
    expert_share = expert_share / jnp.sum(expert_share, axis=-1, keepdims=True)
    route_weight = group_weight[:, None] * expert_share
    mixture = tokens_f + jnp.sum(route_weight[:, :, None] * picked.astype(jnp.float32), axis=1)
    residual = mixture.astype(jnp.bfloat16)
    sliced = lax.all_to_all(residual, "tp", split_axis=1, concat_axis=0, tiled=True).astype(
        jnp.float32
    )
    squares = of_everyone(jnp.sum(sliced * sliced, axis=-1), "tp")
    inverse_out = lax.rsqrt(squares / D + EPS)
    return (sliced * inverse_out[:, None] * final_gain.astype(jnp.float32)).astype(jnp.bfloat16)


def solution(mesh):
    placed = (
        P(("ep", "tp"), None),
        P(),
        P(("ep", "tp"), None),
        P(("ep", "tp")),
        P(("ep", "tp"), None),
        P("ep", None, "tp"),
        P("ep", None, "tp"),
        P("ep", "tp", None),
        P("tp"),
    )
    return jax.shard_map(
        local, mesh=mesh, in_specs=placed, out_specs=P("ep", "tp"), check_vma=False
    )
```

profile of v0, /device:TPU:1, one launch (start us, length us, event | category | flops | bytes accessed | tf_op | source)
XLA Modules:
  0.0 336.0 jit_solution(12380158501986293698)
XLA Ops:
  6.5 3.1 pad_maximum_fusion
  10.3 1.2 reduce-window.6
  12.0 2.4 scatter_custom_fusion
  15.3 6.1 %gather_fusion = bf16[1024,2048]{1,0:T(8,128)(2,1)} fusion(bf16[256,2048]{1,0:T(8,128)(2,1)S(1)} %fusion.9, s32[1024]{0:T(1024)S(1)} %maximum_clamp_fusion), kind=kCustom, calls=%fused_computation | custom fusion | bytes 8392704 | tf_op jit(solution)/shard_map/gather | solution.py:52
  21.3 9.4 %copy_select_fusion = bf16[16,64,2048]{2,0,1:T(8,128)(2,1)} fusion(bf16[16,64,2048]{2,1,0:T(8,128)(2,1)} %bitcast.57, pred[16,64]{0,1:T(8,128)(4,1)S(1)} %copy.60), kind=kLoop, calls=%fused_computation.9 | loop fusion | flops 2097152 | bytes 8389632 | tf_op jit(solution)/shard_map/jit(_where)/select_n | solution.py:53
  30.7 13.3 %all-to-all-start = ((bf16[16,64,2048]{2,0,1:T(8,128)(2,1)}), bf16[16,64,2048]{2,0,1:T(8,128)(2,1)}, u32[]{:S(2)}, u32[]{:S(2)}) async-start(bf16[16,64,2048]{2,0,1:T(8,128)(2,1)} %copy_select_fusion), calls=%async_computation | async-start | bytes 8388608 | tf_op jit(solution)/shard_map/all_to_all | solution.py:58
  44.3 0.5 all-gather.5.cloned.1.call-update
  44.8 94.0 %all-to-all-done = bf16[16,64,2048]{2,0,1:T(8,128)(2,1)} async-done(((bf16[16,64,2048]{2,0,1:T(8,128)(2,1)}), bf16[16,64,2048]{2,0,1:T(8,128)(2,1)}, u32[]{:S(2)}, u32[]{:S(2)}) %all-to-all-start) | async-done | bytes 4194336 | tf_op jit(solution)/shard_map/all_to_all | solution.py:58
  138.8 6.5 %copy.62 = bf16[16,64,2048]{2,1,0:T(8,128)(2,1)} copy(bf16[16,64,2048]{2,0,1:T(8,128)(2,1)} %all-to-all-done) | data formatting | bytes 8388608 | tf_op jit(solution)/shard_map/all_to_all | solution.py:58
  145.3 7.7 %fusion = f32[1024,1024]{1,0:T(8,128)S(1)} fusion(bf16[1024,2048]{1,0:T(8,128)(2,1)} %bitcast.58, bf16[2,2048,1024]{2,1,0:T(8,128)(2,1)} %all-gather.3.cloned.1.call-done), kind=kOutput, calls=%fused_computation.4 | convolution fusion | flops 4294967296 | bytes 12582912 | tf_op jit(solution)/shard_map/dot_general | solution.py:64
  153.0 6.4 %multiply_convert_fusion = bf16[1024,1024]{1,0:T(8,128)(2,1)} fusion(f32[1024,1024]{1,0:T(8,128)S(1)} %fusion, bf16[1024,2048]{1,0:T(8,128)(2,1)S(1)} %bitcast.59, bf16[2,2048,1024]{2,1,0:T(8,128)(2,1)S(1)} %copy-done.7), kind=kOutput, calls=%fused_computation.11 | convolution fusion | flops 4301258752 | bytes 14680064 | tf_op jit(solution)/shard_map/dot_general | solution.py:63
  159.4 7.3 %fusion.4 = bf16[1024,2048]{1,0:T(8,128)(2,1)S(1)} fusion(bf16[1024,1024]{1,0:T(8,128)(2,1)} %multiply_convert_fusion, bf16[1,1024,2048]{2,1,0:T(8,128)(2,1)} %all-gather.5.cloned.1.call-done), kind=kOutput, calls=%fused_computation.12 | convolution fusion | flops 4297064448 | bytes 10485760 | tf_op jit(solution)/shard_map/dot_general | solution.py:66
  166.7 4.3 %copy.63 = bf16[16,64,2048]{2,0,1:T(8,128)(2,1)} copy(bf16[16,64,2048]{2,1,0:T(8,128)(2,1)S(1)} %bitcast.60) | data formatting | bytes 8388608 | tf_op jit(solution)/shard_map/reshape;stack;reshape | solution.py:70
  171.0 7.6 %all-to-all-start.1 = ((bf16[16,64,2048]{2,0,1:T(8,128)(2,1)}), bf16[16,64,2048]{2,0,1:T(8,128)(2,1)}, u32[]{:S(2)}, u32[]{:S(2)}) async-start(bf16[16,64,2048]{2,0,1:T(8,128)(2,1)} %copy.63), calls=%async_computation.1 | async-start | bytes 8388608 | tf_op jit(solution)/shard_map/all_to_all | solution.py:71
  178.8 94.5 %all-to-all-done.1 = bf16[16,64,2048]{2,0,1:T(8,128)(2,1)} async-done(((bf16[16,64,2048]{2,0,1:T(8,128)(2,1)}), bf16[16,64,2048]{2,0,1:T(8,128)(2,1)}, u32[]{:S(2)}, u32[]{:S(2)}) %all-to-all-start.1) | async-done | bytes 4194336 | tf_op jit(solution)/shard_map/all_to_all | solution.py:71
  273.3 6.5 %copy.64 = bf16[16,64,2048]{2,1,0:T(8,128)(2,1)} copy(bf16[16,64,2048]{2,0,1:T(8,128)(2,1)} %all-to-all-done.1) | data formatting | bytes 8388608 | tf_op jit(solution)/shard_map/all_to_all | solution.py:71
  279.8 8.0 %gather_fusion.1 = bf16[512,2048]{1,0:T(8,128)(2,1)} fusion(bf16[1024,2048]{1,0:T(8,128)(2,1)} %bitcast.56, s32[1024]{0:T(1024)S(1)} %pad_clamp_fusion), kind=kCustom, calls=%fused_computation.1 | custom fusion | bytes 4196352 | tf_op jit(solution)/shard_map/gather | solution.py:72
  287.8 5.4 %reshape.98 = f32[256,2,2048]{2,1,0:T(2,128)} reshape(bf16[512,2048]{1,0:T(8,128)(2,1)} %gather_fusion.1) | data formatting | bytes 6291456 | tf_op jit(solution)/shard_map/convert_element_type | solution.py:76
  293.2 8.9 %multiply_reduce_fusion = f32[256,2048]{1,0:T(8,128)S(1)} fusion(f32[256,2,2048]{2,1,0:T(2,128)} %reshape.98, f32[256,2]{1,0:T(8,128)S(1)} %copy.55), kind=kLoop, calls=%fused_computation.10 | loop fusion | flops 1572864 | bytes 6293504 | tf_op jit(solution)/shard_map/reduce_sum | solution.py:76
  302.5 16.8 %all_to_all.29 = bf16[256,4,512]{2,0,1:T(8,128)(2,1)S(1)} all-to-all(bf16[256,4,512]{2,0,1:T(8,128)(2,1)S(1)} %bitcast.61), channel_id=1, replica_groups=mesh['ep'=64,'tp'=4] {'tp'}, dimensions={1} | all-to-all | bytes 2097152 | tf_op jit(solution)/shard_map/all_to_all | solution.py:78
  319.8 0.6 broadcast_in_dim.40
  320.4 3.3 all-to-all-start.3
  323.7 4.2 %all-to-all-done.3 = f32[4,1,1024]{2,1,0:T(1,128)S(1)} async-done(((f32[4,1,1024]{2,1,0:T(1,128)}), f32[4,1,1024]{2,1,0:T(1,128)S(1)}, u32[]{:S(2)}, u32[]{:S(2)}) %all-to-all-start.3) | async-done | bytes 16416 | tf_op jit(solution)/shard_map/all_to_all | solution.py:23
  327.9 1.3 fusion.12
  (54 shorter events, 3.2 us)
Async XLA Ops:
  6.5 3.2 copy-start.4
  6.5 5.3 %copy-start.3 = (bf16[2048]{0:T(1024)(128)(2,1)S(1)}, bf16[2048]{0:T(1024)(128)(2,1)}, u32[]{:S(2)}) copy-start(bf16[2048]{0:T(1024)(128)(2,1)} %param.10) | copy-start | bytes 12292
  6.5 8.1 %copy-start = (bf16[256,2048]{1,0:T(8,128)(2,1)S(1)}, bf16[256,2048]{1,0:T(8,128)(2,1)}, u32[]{:S(2)}) copy-start(bf16[256,2048]{1,0:T(8,128)(2,1)} %param.9) | copy-start | bytes 3145732
  6.5 138.7 %all-gather.3.cloned.1.call-start = ((), (), s32[]{:S(2)}) async-start(), calls=%async_computation.4 | async-start | bytes 10485760 | tf_op jit(solution)/shard_map/all_gather | solution.py:14
  30.7 108.0 %all-to-all-start = ((bf16[16,64,2048]{2,0,1:T(8,128)(2,1)}), bf16[16,64,2048]{2,0,1:T(8,128)(2,1)}, u32[]{:S(2)}, u32[]{:S(2)}) async-start(bf16[16,64,2048]{2,0,1:T(8,128)(2,1)} %copy_select_fusion), calls=%async_computation | async-start | bytes 8388608 | tf_op jit(solution)/shard_map/all_to_all | solution.py:58
  44.1 115.3 %all-gather.5.cloned.1.call-start = ((), (), s32[]{:S(2)}) async-start(), calls=%async_computation.5 | async-start | bytes 5242880 | tf_op jit(solution)/shard_map/all_gather | solution.py:56
  145.3 7.7 %copy-start.1 = (bf16[16,64,2048]{2,1,0:T(8,128)(2,1)S(1)}, bf16[16,64,2048]{2,1,0:T(8,128)(2,1)}, u32[]{:S(2)}) copy-start(bf16[16,64,2048]{2,1,0:T(8,128)(2,1)} %copy.62) | copy-start | bytes 12582916
  145.3 7.7 %copy-start.7 = (bf16[2,2048,1024]{2,1,0:T(8,128)(2,1)S(1)}, bf16[2,2048,1024]{2,1,0:T(8,128)(2,1)}, u32[]{:S(2)}) copy-start(bf16[2,2048,1024]{2,1,0:T(8,128)(2,1)} %all-gather.3.cloned.1.call-done) | copy-start | bytes 25165828
  171.0 7.6 %copy-start.2 = (f32[256,2]{0,1:T(2,128)S(1)}, f32[256,2]{0,1:T(2,128)}, u32[]{:S(2)}) copy-start(f32[256,2]{0,1:T(2,128)} %param.13) | copy-start | bytes 6148
  171.0 7.7 %copy-start.6 = (f32[256]{0:T(256)S(1)}, f32[256]{0:T(256)}, u32[]{:S(2)}) copy-start(f32[256]{0:T(256)} %param.12) | copy-start | bytes 3076
  171.0 102.3 %all-to-all-start.1 = ((bf16[16,64,2048]{2,0,1:T(8,128)(2,1)}), bf16[16,64,2048]{2,0,1:T(8,128)(2,1)}, u32[]{:S(2)}, u32[]{:S(2)}) async-start(bf16[16,64,2048]{2,0,1:T(8,128)(2,1)} %copy.63), calls=%async_computation.1 | async-start | bytes 8388608 | tf_op jit(solution)/shard_map/all_to_all | solution.py:71
  302.1 21.6 %copy-start.5 = (bf16[512]{0:T(512)(128)(2,1)S(1)}, bf16[512]{0:T(512)(128)(2,1)}, u32[]{:S(2)}) copy-start(bf16[512]{0:T(512)(128)(2,1)} %param.17) | copy-start | bytes 3076
  320.4 7.4 %all-to-all-start.3 = ((f32[4,1,1024]{2,1,0:T(1,128)}), f32[4,1,1024]{2,1,0:T(1,128)S(1)}, u32[]{:S(2)}, u32[]{:S(2)}) async-start(f32[4,1,1024]{2,1,0:T(1,128)} %broadcast_in_dim.40), calls=%async_computation.3 | async-start | bytes 32768 | tf_op jit(solution)/shard_map/all_to_all | solution.py:23
Sparse Core Ops, SparseCore 0:
  9.8 91.3 all-gather.2
  103.1 52.7 all-gather.4
where the time goes:
time: 340 us; the launch traced here: 336 us
  waiting for transfers between devices  193 us (57%)
  local copies, waits for them, and re-layouts  41.2 us (12%)
  other arithmetic  25.4 us (7%)
  starting transfers between devices  24.4 us (7%)
  matrix products  21.4 us (6%)
  blocking collectives  16.8 us (5%)
  between operations  13.7 us (4%)
    all_to_all x1, waiting for transfers between devices, local(): lax.all_to_all(answer, 'ep', split_axis=1, concat_axis=1, tiled=True)  94.5 us
    all_to_all x1, waiting for transfers between devices, local(): lax.all_to_all(outgoing, 'ep', split_axis=1, concat_axis=1, tiled=True)  94 us
    all_to_all x1, blocking collectives, local(): lax.all_to_all(residual, 'tp', split_axis=1, concat_axis=0, tiled=True)  16.8 us
    all_to_all x1, starting transfers between devices, local(): lax.all_to_all(outgoing, 'ep', split_axis=1, concat_axis=1, tiled=True)  13.3 us
    select_n x1, other arithmetic, local(): jnp.where((owner_row > 0)[:, None], source, jnp.zeros_like(source))  9.42 us
    reduce_sum x1, other arithmetic, local(): jnp.sum(route_weight[:, :, None] * picked.astype(jnp.float32), axis=1)  8.89 us
    gather x1, local copies, waits for them, and re-layouts, local(): arrived.reshape(capacity * experts, width)[position]  7.96 us
    dot_general x1, matrix products, local(): up_full = jnp.dot(routed, up_whole[0], preferred_element_type=jnp.float32)  7.69 us
  transfers between devices with their start and end apart: 5, of which 3 were waited for; matrix products, arithmetic and copies ran while one was open for 12% of the time, Pallas kernels for 0%

commit v1 on v0

v1 whole, which is shorter than its diff:
```python
import jax
import jax.numpy as jnp
from jax import lax
from jax.sharding import PartitionSpec as P

D = 2048
CAP = 16
EPS = 1e-06


def local(
    tokens, norm_gain, expert_ids, group_weight, expert_logit, w_gate, w_up, w_down, final_gain
):
    rows, width = tokens.shape
    experts = lax.axis_size("ep")
    slots = experts * CAP
    down_whole = lax.all_gather(w_down, "tp", axis=1, tiled=True)[0]
    both = lax.all_gather(jnp.concatenate((w_gate, w_up), axis=0), "tp", axis=2, tiled=True)
    tokens_f = tokens.astype(jnp.float32)
    inverse_in = lax.rsqrt(jnp.mean(tokens_f * tokens_f, axis=-1, keepdims=True) + EPS)
    normed_in = (tokens_f * inverse_in * norm_gain.astype(jnp.float32)).astype(jnp.bfloat16)
    lane = jnp.arange(experts, dtype=jnp.int32)[None, :]
    first = expert_ids[:, 0:1] == lane
    second = expert_ids[:, 1:2] == lane
    named = (first | second).astype(jnp.bfloat16)
    order = jnp.arange(rows, dtype=jnp.int32)
    earlier = (order[:, None] > order[None, :]).astype(jnp.bfloat16)
    before = jnp.dot(earlier, named, preferred_element_type=jnp.float32)
    rank0 = jnp.sum(jnp.where(first, before, 0.0), axis=1).astype(jnp.int32)
    rank1 = jnp.sum(jnp.where(second, before, 0.0), axis=1).astype(jnp.int32)
    at0 = expert_ids[:, 0] * CAP + rank0
    at1 = expert_ids[:, 1] * CAP + rank1
    slot = jnp.arange(slots, dtype=jnp.int32)
    pick = ((slot[:, None] == at0[None, :]) | (slot[:, None] == at1[None, :])).astype(jnp.bfloat16)
    outgoing = jnp.dot(pick, normed_in, preferred_element_type=jnp.float32).astype(jnp.bfloat16)
    incoming = lax.all_to_all(
        outgoing.reshape(experts, CAP, width), "ep", split_axis=0, concat_axis=0, tiled=True
    )
    routed = incoming.reshape(slots, width)
    gate_full = jnp.dot(routed, both[0], preferred_element_type=jnp.float32)
    up_full = jnp.dot(routed, both[1], preferred_element_type=jnp.float32)
    hidden = (jax.nn.silu(gate_full) * up_full).astype(jnp.bfloat16)
    product = jnp.dot(hidden, down_whole, preferred_element_type=jnp.float32).astype(jnp.bfloat16)
    arrived = lax.all_to_all(
        product.reshape(experts, CAP, width), "ep", split_axis=0, concat_axis=0, tiled=True
    ).reshape(slots, width)
    share = jnp.exp(expert_logit)
    weight = group_weight[:, None] * (share / jnp.sum(share, axis=-1, keepdims=True))
    spread = jnp.where(slot[None, :] == at0[:, None], weight[:, 0:1], 0.0) + jnp.where(
        slot[None, :] == at1[:, None], weight[:, 1:2], 0.0
    )
    high = spread.astype(jnp.bfloat16)
    low = (spread - high.astype(jnp.float32)).astype(jnp.bfloat16)
    mixed = jnp.dot(high, arrived, preferred_element_type=jnp.float32) + jnp.dot(
        low, arrived, preferred_element_type=jnp.float32
    )
    residual = (tokens_f + mixed).astype(jnp.bfloat16)
    pieces = residual.reshape(rows, 4, width // 4).transpose(1, 0, 2)
    sliced = lax.all_to_all(pieces, "tp", split_axis=0, concat_axis=0, tiled=True)
    sliced = sliced.reshape(4 * rows, width // 4).astype(jnp.float32)
    squares = lax.all_gather(jnp.sum(sliced * sliced, axis=-1), "tp", axis=0).sum(axis=0)
    inverse_out = lax.rsqrt(squares / D + EPS)
    return (sliced * inverse_out[:, None] * final_gain.astype(jnp.float32)).astype(jnp.bfloat16)


def solution(mesh):
    placed = (
        P(("ep", "tp"), None),
        P(),
        P(("ep", "tp"), None),
        P(("ep", "tp")),
        P(("ep", "tp"), None),
        P("ep", None, "tp"),
        P("ep", None, "tp"),
        P("ep", "tp", None),
        P("tp"),
    )
    return jax.shard_map(
        local, mesh=mesh, in_specs=placed, out_specs=P("ep", "tp"), check_vma=False
    )
```

time: 340 us -> 317 us (0.932)
  local copies, waits for them, and re-layouts: 41.2 us -> 1.12 us
  waiting for transfers between devices: 193 us -> 221 us
  other arithmetic: 25.4 us -> 5.08 us
  matrix products: 21.4 us -> 34.3 us
  blocking collectives: 16.8 us -> 9.13 us
  starting transfers between devices: 24.4 us -> 27.9 us
    all_gather x2, waiting for transfers between devices: 0.01 us -> 19.1 us  [the longest x1 19.1 us: local(): down_whole = lax.all_gather(w_down, 'tp', axis=1, tiled=True)[0]]
    all_to_all x1 -> x0, blocking collectives: 16.8 us -> none  [local(): lax.all_to_all(residual, 'tp', split_axis=1, concat_axis=0, tiled=True)]
    gather x2 -> x0, local copies, waits for them, and re-layouts: 14 us -> none  [the longest x1 7.96 us: local(): arrived.reshape(capacity * experts, width)[position]]
    all_to_all x3 -> x0, local copies, waits for them, and re-layouts: 13 us -> none  [the longest x1 6.47 us: local(): lax.all_to_all(outgoing, 'ep', split_axis=1, concat_axis=1, tiled=True)]
    dot_general x3 -> x7, matrix products: 21.4 us -> 34.3 us  [the longest x1 8.2 us: local(): jnp.dot(hidden, down_whole, preferred_element_type=jnp.float32)]
    select_n x2 -> x0, other arithmetic: 9.42 us -> none  [the longest x1 9.42 us: local(): jnp.where((owner_row > 0)[:, None], source, jnp.zeros_like(source))]
    all_gather x0 -> x1, blocking collectives: none -> 9.13 us  [local(): lax.all_gather(jnp.sum(sliced * sliced, axis=-1), 'tp', axis=0).sum(axis=0)]
    reduce_sum x5 -> x3, other arithmetic: 9.33 us -> 0.32 us  [the longest x1 0.28 us: local(): jnp.sum(sliced * sliced, axis=-1)]
  transfers between devices with their start and end apart: 5 -> 5, of which waited for: 3 -> 4; matrix products, arithmetic and copies ran while one was open for 12% -> 6% of each run, Pallas kernels for 0% -> 0%
where the time goes in v1:
time: 317 us; the launch traced here: 313 us
  waiting for transfers between devices  221 us (70%)
  matrix products  34.3 us (11%)
  starting transfers between devices  27.9 us (9%)
  between operations  13.6 us (4%)
  blocking collectives  9.13 us (3%)
  other arithmetic  5.08 us (2%)
    all_to_all x1, waiting for transfers between devices, local(): lax.all_to_all(product.reshape(experts, CAP, width), 'ep', split_axis=0,...  94.6 us
    all_to_all x1, waiting for transfers between devices, local(): lax.all_to_all(outgoing.reshape(experts, CAP, width), 'ep', split_axis=0,...  94 us
    all_gather x1, waiting for transfers between devices, local(): down_whole = lax.all_gather(w_down, 'tp', axis=1, tiled=True)[0]  19.1 us
    all_to_all x1, starting transfers between devices, local(): lax.all_to_all(outgoing.reshape(experts, CAP, width), 'ep', split_axis=0,...  13.2 us
    all_to_all x1, waiting for transfers between devices, local(): lax.all_to_all(pieces, 'tp', split_axis=0, concat_axis=0, tiled=True)  13 us
    all_to_all x1, starting transfers between devices, local(): lax.all_to_all(product.reshape(experts, CAP, width), 'ep', split_axis=0,...  11.2 us
    all_gather x1, blocking collectives, local(): lax.all_gather(jnp.sum(sliced * sliced, axis=-1), 'tp', axis=0).sum(axis=0)  9.13 us
    dot_general x1, matrix products, local(): jnp.dot(hidden, down_whole, preferred_element_type=jnp.float32)  8.2 us
  transfers between devices with their start and end apart: 5, of which 4 were waited for; matrix products, arithmetic and copies ran while one was open for 6% of the time, Pallas kernels for 0%

profile of v1, /device:TPU:1, one launch (start us, length us, event | category | flops | bytes accessed | tf_op | source)
XLA Modules:
  0.0 312.6 jit_solution(2494651620982889680)
XLA Ops:
  6.5 3.1 %pad_maximum_fusion = bf16[2,2048,256]{2,1,0:T(8,128)(2,1)} fusion(bf16[1,2048,256]{2,1,0:T(8,128)(2,1)} %param.15, bf16[1,2048,256]{2,1,0:T(8,128)(2,1)} %param.14), kind=kLoop, calls=%fused_computation.17 | loop fusion | flops 1048576 | bytes 4194304 | tf_op jit(solution)/shard_map/concatenate | solution.py:18
  9.7 0.0 all-gather.4.cloned.1.call-update
  9.7 0.2 select_reduce_fusion.1
  10.0 0.3 fusion.8
  10.3 3.3 %convolution_convert_fusion = bf16[1024,2048]{1,0:T(8,128)(2,1)} fusion(bf16[256,2048]{1,0:T(8,128)(2,1)S(1)} %copy-done, f32[2048]{0:T(1024)S(1)} %convert_element_type.88, f32[256]{0:T(256)S(1)} %add_rsqrt_fusion.1, s32[256]{0:T(256)S(1)} %get-tuple-element.13, s32[256]{0:T(256)S(1)} %get-tuple-element.14), kind=kOutput, calls=%fused_computation.7 | convolution fusion | flops 1078722560 | bytes 5254144 | tf_op jit(solution)/shard_map/dot_general | solution.py:35
  13.6 13.2 %all-to-all-start = ((bf16[64,16,2048]{2,1,0:T(8,128)(2,1)}), bf16[64,16,2048]{2,1,0:T(8,128)(2,1)}, u32[]{:S(2)}, u32[]{:S(2)}) async-start(bf16[64,16,2048]{2,1,0:T(8,128)(2,1)} %bitcast.43), calls=%async_computation | async-start | bytes 8388608 | tf_op jit(solution)/shard_map/all_to_all | solution.py:36
  26.8 0.0 all-gather.6.cloned.1.call-start
  26.8 0.7 all-gather.6.cloned.1.call-update
  27.5 94.0 %all-to-all-done = bf16[64,16,2048]{2,1,0:T(8,128)(2,1)} async-done(((bf16[64,16,2048]{2,1,0:T(8,128)(2,1)}), bf16[64,16,2048]{2,1,0:T(8,128)(2,1)}, u32[]{:S(2)}, u32[]{:S(2)}) %all-to-all-start) | async-done | bytes 4194336 | tf_op jit(solution)/shard_map/all_to_all | solution.py:36
  121.5 7.6 %fusion = f32[1024,1024]{1,0:T(8,128)S(1)} fusion(bf16[1024,2048]{1,0:T(8,128)(2,1)} %bitcast.9, bf16[2,2048,1024]{2,1,0:T(8,128)(2,1)} %all-gather.4.cloned.1.call-done), kind=kOutput, calls=%fused_computation.1 | convolution fusion | flops 4294967296 | bytes 12582912 | tf_op jit(solution)/shard_map/dot_general | solution.py:41
  129.2 7.6 %multiply_convert_fusion = bf16[1024,1024]{1,0:T(8,128)(2,1)S(1)} fusion(f32[1024,1024]{1,0:T(8,128)S(1)} %fusion, bf16[1024,2048]{1,0:T(8,128)(2,1)} %bitcast.9, bf16[2,2048,1024]{2,1,0:T(8,128)(2,1)S(1)} %copy-done.6), kind=kOutput, calls=%fused_computation.6 | convolution fusion | flops 4301258752 | bytes 14680064 | tf_op jit(solution)/shard_map/dot_general | solution.py:40
  136.7 19.1 %all-gather.6.cloned.1.call-done = bf16[1,1024,2048]{2,1,0:T(8,128)(2,1)} async-done(((bf16[1,256,2048]{2,1,0:T(8,128)(2,1)}), bf16[1,1024,2048]{2,1,0:T(8,128)(2,1)}) %all-gather.6.cloned.1.call-update) | async-done | bytes 4194320 | tf_op jit(solution)/shard_map/all_gather | solution.py:17
  155.9 8.2 %fusion.4 = bf16[1024,2048]{1,0:T(8,128)(2,1)} fusion(bf16[1024,1024]{1,0:T(8,128)(2,1)S(1)} %multiply_convert_fusion, bf16[1,1024,2048]{2,1,0:T(8,128)(2,1)} %all-gather.6.cloned.1.call-done), kind=kOutput, calls=%fused_computation.8 | convolution fusion | flops 4297064448 | bytes 10485760 | tf_op jit(solution)/shard_map/dot_general | solution.py:43
  164.1 11.2 %all-to-all-start.1 = ((bf16[64,16,2048]{2,1,0:T(8,128)(2,1)}), bf16[64,16,2048]{2,1,0:T(8,128)(2,1)}, u32[]{:S(2)}, u32[]{:S(2)}) async-start(bf16[64,16,2048]{2,1,0:T(8,128)(2,1)} %bitcast.44), calls=%async_computation.1 | async-start | bytes 8388608 | tf_op jit(solution)/shard_map/all_to_all | solution.py:44
  175.3 94.6 %all-to-all-done.1 = bf16[64,16,2048]{2,1,0:T(8,128)(2,1)} async-done(((bf16[64,16,2048]{2,1,0:T(8,128)(2,1)}), bf16[64,16,2048]{2,1,0:T(8,128)(2,1)}, u32[]{:S(2)}, u32[]{:S(2)}) %all-to-all-start.1) | async-done | bytes 4194336 | tf_op jit(solution)/shard_map/all_to_all | solution.py:44
  269.9 3.7 %fusion.27 = f32[256,2048]{1,0:T(8,128)S(1)} fusion(bf16[1024,2048]{1,0:T(8,128)(2,1)} %bitcast.14, f32[256]{0:T(256)S(1)} %bitcast.54, s32[256]{0:T(256)S(1)} %bitcast.58, f32[256]{0:T(256)S(1)} %bitcast.52, s32[256]{0:T(256)S(1)} %bitcast.56), kind=kOutput, calls=%fused_computation.40 | convolution fusion | flops 1075314688 | bytes 6295552 | tf_op jit(solution)/shard_map/dot_general | solution.py:54
  273.6 3.7 %fusion.7 = bf16[256,2048]{1,0:T(8,128)(2,1)S(1)} fusion(f32[256,2048]{1,0:T(8,128)S(1)} %fusion.27, bf16[1024,2048]{1,0:T(8,128)(2,1)} %bitcast.14, bf16[256,2048]{1,0:T(8,128)(2,1)S(1)} %copy-done, f32[256]{0:T(256)S(1)} %bitcast.55, s32[256]{0:T(256)S(1)} %bitcast.59, f32[256]{0:T(256)S(1)} %bitcast.53, s32[256]{0:T(256)S(1)} %bitcast.57), kind=kOutput, calls=%fused_computation.13 | convolution fusion | flops 1078198272 | bytes 8392704 | tf_op jit(solution)/shard_map/dot_general | solution.py:54
  277.3 0.0 copy-start.4
  277.3 1.1 copy.19
  278.4 3.5 %all-to-all-start.2 = ((bf16[4,256,512]{2,1,0:T(8,128)(2,1)}), bf16[4,256,512]{2,1,0:T(8,128)(2,1)S(1)}, u32[]{:S(2)}, u32[]{:S(2)}) async-start(bf16[4,256,512]{2,1,0:T(8,128)(2,1)} %bitcast.42), calls=%async_computation.2 | async-start | bytes 2097152 | tf_op jit(solution)/shard_map/all_to_all | solution.py:59
  281.9 13.0 %all-to-all-done.2 = bf16[4,256,512]{2,1,0:T(8,128)(2,1)S(1)} async-done(((bf16[4,256,512]{2,1,0:T(8,128)(2,1)}), bf16[4,256,512]{2,1,0:T(8,128)(2,1)S(1)}, u32[]{:S(2)}, u32[]{:S(2)}) %all-to-all-start.2) | async-done | bytes 1048608 | tf_op jit(solution)/shard_map/all_to_all | solution.py:59
  295.0 0.3 multiply_reduce_fusion
  295.3 9.1 %all-gather = f32[4,1,1024]{2,1,0:T(1,128)S(1)} all-gather(f32[1,1,1024]{2,1,0:T(1,128)S(1)} %reshape.77), channel_id=1, replica_groups=mesh['ep'=64,'tp'=4] {'tp'}, dimensions={0}, use_global_device_ids=true | all-gather | bytes 20480 | tf_op jit(solution)/shard_map/all_gather | solution.py:61
  304.4 1.3 fusion.12
  (29 shorter events, 0.2 us)
Async XLA Ops:
  6.5 3.2 %copy-start.3 = (bf16[2048]{0:T(1024)(128)(2,1)S(1)}, bf16[2048]{0:T(1024)(128)(2,1)}, u32[]{:S(2)}) copy-start(bf16[2048]{0:T(1024)(128)(2,1)} %param.10) | copy-start | bytes 12292
  6.5 3.2 %copy-start.2 = (s32[256,2]{0,1:T(2,128)S(1)}, s32[256,2]{0,1:T(2,128)}, u32[]{:S(2)}) copy-start(s32[256,2]{0,1:T(2,128)} %param.11) | copy-start | bytes 6148
  6.5 3.4 %copy-start = (bf16[256,2048]{1,0:T(8,128)(2,1)S(1)}, bf16[256,2048]{1,0:T(8,128)(2,1)}, u32[]{:S(2)}) copy-start(bf16[256,2048]{1,0:T(8,128)(2,1)} %param.9) | copy-start | bytes 3145732
  6.5 115.0 %all-gather.4.cloned.1.call-start = ((), (), s32[]{:S(2)}) async-start(), calls=%async_computation.3 | async-start | bytes 10485760 | tf_op jit(solution)/shard_map/all_gather | solution.py:18
  13.6 107.9 %all-to-all-start = ((bf16[64,16,2048]{2,1,0:T(8,128)(2,1)}), bf16[64,16,2048]{2,1,0:T(8,128)(2,1)}, u32[]{:S(2)}, u32[]{:S(2)}) async-start(bf16[64,16,2048]{2,1,0:T(8,128)(2,1)} %bitcast.43), calls=%async_computation | async-start | bytes 8388608 | tf_op jit(solution)/shard_map/all_to_all | solution.py:36
  26.8 129.1 %all-gather.6.cloned.1.call-start = ((), (), s32[]{:S(2)}) async-start(), calls=%async_computation.4 | async-start | bytes 5242880 | tf_op jit(solution)/shard_map/all_gather | solution.py:17
  121.5 7.7 %copy-start.6 = (bf16[2,2048,1024]{2,1,0:T(8,128)(2,1)S(1)}, bf16[2,2048,1024]{2,1,0:T(8,128)(2,1)}, u32[]{:S(2)}) copy-start(bf16[2,2048,1024]{2,1,0:T(8,128)(2,1)} %all-gather.4.cloned.1.call-done) | copy-start | bytes 25165828
  164.1 11.2 %copy-start.1 = (f32[256,2]{0,1:T(2,128)S(1)}, f32[256,2]{0,1:T(2,128)}, u32[]{:S(2)}) copy-start(f32[256,2]{0,1:T(2,128)} %param.13) | copy-start | bytes 6148
  164.1 11.2 %copy-start.5 = (f32[256]{0:T(256)S(1)}, f32[256]{0:T(256)}, u32[]{:S(2)}) copy-start(f32[256]{0:T(256)} %param.12) | copy-start | bytes 3076
  164.1 105.9 %all-to-all-start.1 = ((bf16[64,16,2048]{2,1,0:T(8,128)(2,1)}), bf16[64,16,2048]{2,1,0:T(8,128)(2,1)}, u32[]{:S(2)}, u32[]{:S(2)}) async-start(bf16[64,16,2048]{2,1,0:T(8,128)(2,1)} %bitcast.44), calls=%async_computation.1 | async-start | bytes 8388608 | tf_op jit(solution)/shard_map/all_to_all | solution.py:44
  277.3 4.6 %copy-start.4 = (bf16[512]{0:T(512)(128)(2,1)S(1)}, bf16[512]{0:T(512)(128)(2,1)}, u32[]{:S(2)}) copy-start(bf16[512]{0:T(512)(128)(2,1)} %param.17) | copy-start | bytes 3076
  278.4 16.6 %all-to-all-start.2 = ((bf16[4,256,512]{2,1,0:T(8,128)(2,1)}), bf16[4,256,512]{2,1,0:T(8,128)(2,1)S(1)}, u32[]{:S(2)}, u32[]{:S(2)}) async-start(bf16[4,256,512]{2,1,0:T(8,128)(2,1)} %bitcast.42), calls=%async_computation.2 | async-start | bytes 2097152 | tf_op jit(solution)/shard_map/all_to_all | solution.py:59
Sparse Core Ops, SparseCore 0:
  9.8 91.3 all-gather.3
  103.1 52.7 all-gather.5

commit v2 on v1

v2 whole, which is shorter than its diff:
```python
import functools

import jax
import jax.numpy as jnp
from jax import lax
from jax.experimental import pallas as pl
from jax.experimental.pallas import tpu as pltpu
from jax.sharding import PartitionSpec as P

D = 2048
FF = 1024
CAP = 16
ROWS = 256
PLANES = 8
GROUP = 8
LANES = GROUP * CAP
TP = 4
EPS = 1e-06
MESH = pl.DeviceIdType.MESH
F32 = jnp.float32
BF16 = jnp.bfloat16


def plane_step(i):
    return 4 + (1 - 2 * (i % 2)) * ((i + 1) // 2)


def kernel(
    tokens, gain, ids, group_weight, logit, w_gate, w_up, w_down, final_gain, out,
    normed, packed, routed, hidden, product, returned, wg, wu, wd, high, low, mixed,
    gains, result, finished,
    own_sem, w_send, w_recv, gain_send, gain_recv, out_send, out_recv, back_send, back_recv,
    last_send, last_recv,
):
    ep, tp = lax.axis_index("ep"), lax.axis_index("tp")
    z, inner = ep // GROUP, ep % GROUP
    x, core = inner // 2, inner % 2
    right, left, opposite = (tp + 1) % TP, (tp + 3) % TP, (tp + 2) % TP

    def peer(i):
        step, j = i // GROUP, (i + 1) % GROUP
        pz = (z + plane_step(step)) % PLANES
        return pz * GROUP + ((x + j // 2) % 4) * 2 + (core + j % 2) % 2

    barrier = pltpu.get_barrier_semaphore()

    def greet(i, _):
        pl.semaphore_signal(barrier, inc=1, device_id={"ep": peer(i), "tp": tp}, device_id_type=MESH)
        return 0

    lax.fori_loop(0, 63, greet, 0)
    for other in (right, left, opposite):
        pl.semaphore_signal(barrier, inc=1, device_id={"ep": ep, "tp": other}, device_id_type=MESH)

    own = [
        pltpu.make_async_copy(w_gate, wg.at[tp], own_sem.at[0]),
        pltpu.make_async_copy(w_up, wu.at[tp], own_sem.at[1]),
        pltpu.make_async_copy(w_down, wd.at[tp], own_sem.at[2]),
    ]
    for copy in own:
        copy.start()

    def norm_rows(i, _):
        at = pl.ds(pl.multiple_of(i * 32, 32), 32)
        t = tokens[at, :].astype(F32)
        inverse = lax.rsqrt(jnp.mean(t * t, axis=-1, keepdims=True) + EPS)
        normed[at, :] = (t * inverse * gain[...].astype(F32)).astype(BF16)
        return 0

    lax.fori_loop(0, ROWS // 32, norm_rows, 0)

    id0, id1 = ids[0:1, :], ids[1:2, :]
    lane = lax.broadcasted_iota(jnp.int32, (PLANES * GROUP, ROWS), 0)
    first, second = lane == id0, lane == id1
    named = jnp.where(first, 1.0, jnp.where(second, 1.0, 0.0)).astype(BF16)
    earlier = jnp.where(
        lax.broadcasted_iota(jnp.int32, (ROWS, ROWS), 0)
        < lax.broadcasted_iota(jnp.int32, (ROWS, ROWS), 1), 1.0, 0.0,
    ).astype(BF16)
    before = jnp.dot(named, earlier, preferred_element_type=F32)
    rank0 = jnp.sum(jnp.where(first, before, 0.0), axis=0, keepdims=True)
    rank1 = jnp.sum(jnp.where(second, before, 0.0), axis=0, keepdims=True)
    at0 = id0.astype(F32) * CAP + rank0
    at1 = id1.astype(F32) * CAP + rank1
    slot = lax.broadcasted_iota(jnp.int32, (LANES, ROWS), 0).astype(F32)

    def pack(p, _):
        base = (p * LANES).astype(F32)
        pick = jnp.where(slot == at0 - base, 1.0, jnp.where(slot == at1 - base, 1.0, 0.0)).astype(BF16)
        for n in range(4):
            rows = jnp.dot(pick, normed[:, n * 512:(n + 1) * 512], preferred_element_type=F32)
            packed[pl.ds(p * GROUP, GROUP), :, n * 512:(n + 1) * 512] = rows.astype(BF16).reshape(GROUP, CAP, 512)
        return 0

    lax.fori_loop(0, PLANES, pack, 0)

    for copy in own:
        copy.wait()
    pl.semaphore_wait(barrier, 66)

    def weights(src, dst, sem, to):
        copy = pltpu.make_async_remote_copy(
            src_ref=src, dst_ref=dst, send_sem=w_send.at[sem], recv_sem=w_recv.at[sem],
            device_id={"ep": ep, "tp": to}, device_id_type=MESH,
        )
        copy.start()
        return copy

    half = FF // TP // 2
    top, bottom = pl.ds(0, half), pl.ds(half, half)
    flights = [
        weights(wg.at[tp], wg.at[tp], 0, right),
        weights(wu.at[tp], wu.at[tp], 1, left),
        weights(wu.at[tp], wu.at[tp], 2, right),
        weights(wg.at[tp], wg.at[tp], 3, left),
    ]

    def dispatch(i, _):
        to = peer(i)
        pltpu.make_async_remote_copy(
            src_ref=packed.at[to], dst_ref=routed.at[ep], send_sem=out_send, recv_sem=out_recv.at[z],
            device_id={"ep": to, "tp": tp}, device_id_type=MESH,
        ).start()
        return 0

    lax.fori_loop(0, 63, dispatch, 0)
    routed[ep] = packed[ep]

    gains[tp] = final_gain[...]
    for k, other in enumerate((right, left, opposite)):
        flights.append(pltpu.make_async_remote_copy(
            src_ref=final_gain, dst_ref=gains.at[tp], send_sem=gain_send.at[k], recv_sem=gain_recv.at[k],
            device_id={"ep": ep, "tp": other}, device_id_type=MESH,
        ))
        flights[-1].start()

    e0, e1 = jnp.exp(logit[0:1, :]), jnp.exp(logit[1:2, :])
    total = e0 + e1
    weight0 = group_weight[...] * (e0 / total)
    weight1 = group_weight[...] * (e1 / total)

    def spread(p, _):
        base = (p * LANES).astype(F32)
        w = jnp.where(slot == at0 - base, weight0, 0.0) + jnp.where(slot == at1 - base, weight1, 0.0)
        w = w.T
        top_term = w.astype(BF16)
        high[p] = top_term
        low[p] = (w - top_term.astype(F32)).astype(BF16)
        return 0

    lax.fori_loop(0, PLANES, spread, 0)

    flights[0].wait_recv()
    flights.append(weights(wg.at[left], wg.at[left], 4, right))
    flights[1].wait_recv()
    flights.append(weights(wu.at[right], wu.at[right], 5, left))
    downs = [
        weights(wd.at[tp, top], wd.at[tp, top], 6, right),
        weights(wd.at[tp, bottom], wd.at[tp, bottom], 7, left),
        weights(wd.at[tp, bottom], wd.at[tp, bottom], 8, right),
        weights(wd.at[tp, top], wd.at[tp, top], 9, left),
    ]
    flights[2].wait_recv()
    flights[3].wait_recv()
    flights[-2].wait_recv()
    flights[-1].wait_recv()

    def rows_of(p, count, dst, sem, at):
        pltpu.make_async_remote_copy(
            src_ref=packed.at[pl.ds(0, count)], dst_ref=dst.at[pl.ds(0, count)], send_sem=out_send,
            recv_sem=sem.at[at], device_id={"ep": ep, "tp": right}, device_id_type=MESH,
        ).wait_recv()

    def expand_plane(p):
        xs = routed[pl.ds(p * GROUP, GROUP)].reshape(LANES, D)

        def piece(q, _):
            g = jnp.dot(xs, wg[q], preferred_element_type=F32)
            u = jnp.dot(xs, wu[q], preferred_element_type=F32)
            hidden[p, q] = (g / (1.0 + jnp.exp(-g)) * u).astype(BF16)
            return 0

        lax.fori_loop(0, TP, piece, 0)

    def expand(i, _):
        p = (z + PLANES - plane_step(i)) % PLANES
        rows_of(p, GROUP, routed, out_recv, p)
        expand_plane(p)
        return 0

    lax.fori_loop(0, 4, expand, 0)
    downs[0].wait_recv()
    downs.append(weights(wd.at[left, top], wd.at[left, top], 10, right))
    downs[1].wait_recv()
    downs.append(weights(wd.at[right, bottom], wd.at[right, bottom], 11, left))
    lax.fori_loop(4, 7, expand, 0)
    rows_of(z, GROUP - 1, routed, out_recv, z)
    expand_plane(z)
    for copy in downs[2:]:
        copy.wait_recv()

    def contract_plane(p):
        for n in range(4):
            cols = slice(n * 512, (n + 1) * 512)
            total_rows = jnp.dot(hidden[p, 0], wd[0, :, cols], preferred_element_type=F32)
            for q in range(1, TP):
                total_rows += jnp.dot(hidden[p, q], wd[q, :, cols], preferred_element_type=F32)
            product[pl.ds(p * GROUP, GROUP), :, cols] = total_rows.astype(BF16).reshape(GROUP, CAP, 512)

    def answer(i, _):
        to = peer(i)
        pltpu.make_async_remote_copy(
            src_ref=product.at[to], dst_ref=returned.at[ep], send_sem=back_send, recv_sem=back_recv.at[z],
            device_id={"ep": to, "tp": tp}, device_id_type=MESH,
        ).start()
        return 0

    def contract(i, _):
        contract_plane((z + PLANES - plane_step(i)) % PLANES)
        return 0

    for begin, end in ((0, 1), (1, 3), (3, 5), (5, 7), (7, 8)):
        lax.fori_loop(begin, end, contract, 0)
        lax.fori_loop(begin * GROUP, min(end * GROUP, 63), answer, 0)
    returned[ep] = product[ep]

    def combine_plane(p):
        rows = returned[pl.ds(p * GROUP, GROUP)].reshape(LANES, D)
        for n in range(4):
            cols = slice(n * 512, (n + 1) * 512)
            mixed[:, cols] += jnp.dot(high[p], rows[:, cols], preferred_element_type=F32) + jnp.dot(
                low[p], rows[:, cols], preferred_element_type=F32
            )

    def combine(i, _):
        p = (z + PLANES - plane_step(i)) % PLANES
        rows_of(p, GROUP, returned, back_recv, p)
        combine_plane(p)
        return 0

    mixed[...] = tokens[...].astype(F32)
    lax.fori_loop(0, 7, combine, 0)
    rows_of(z, GROUP - 1, returned, back_recv, z)
    combine_plane(z)

    for k, copy in enumerate(flights[4:7]):
        copy.wait_recv()

    def close(i, _):
        at = pl.ds(pl.multiple_of(i * 32, 32), 32)
        r = mixed[at, :].astype(BF16).astype(F32)
        inverse = lax.rsqrt(jnp.mean(r * r, axis=-1, keepdims=True) + EPS)
        for n in range(TP):
            result[n, at, :] = (r[:, n * 512:(n + 1) * 512] * inverse * gains[n, 0:1, :]).astype(BF16)
        return 0

    lasts = []
    for part in range(4):
        lax.fori_loop(part * 2, part * 2 + 2, close, 0)
        at = pl.ds(part * 64, 64)
        for k, other in enumerate((right, left, opposite)):
            copy = pltpu.make_async_remote_copy(
                src_ref=result.at[other, at], dst_ref=finished.at[tp, at], send_sem=last_send.at[part, k],
                recv_sem=last_recv.at[part, k], device_id={"ep": ep, "tp": other}, device_id_type=MESH,
            )
            copy.start()
            lasts.append(copy)
    out[tp] = result[tp]
    for copy in lasts:
        copy.wait_recv()
    for other in (right, left, opposite):
        out[other] = finished[other]

    for copy in flights + downs + lasts:
        copy.wait_send()
    for sem, src in ((out_send, packed), (back_send, product)):
        pltpu.make_async_remote_copy(
            src_ref=src.at[pl.ds(0, 63)], dst_ref=routed.at[pl.ds(0, 63)], send_sem=sem, recv_sem=out_recv.at[0],
            device_id={"ep": ep, "tp": right}, device_id_type=MESH,
        ).wait_send()


def local(
    tokens, norm_gain, expert_ids, group_weight, expert_logit, w_gate, w_up, w_down, final_gain
):
    vmem = pl.BlockSpec(memory_space=pltpu.VMEM)
    anywhere = pl.BlockSpec(memory_space=pl.ANY)
    dma, groups = pltpu.SemaphoreType.DMA, PLANES * GROUP
    out = pl.pallas_call(
        kernel,
        out_shape=jax.ShapeDtypeStruct((TP, ROWS, D // TP), BF16),
        in_specs=[vmem] * 5 + [anywhere] * 3 + [vmem],
        out_specs=vmem,
        scratch_shapes=[
            pltpu.VMEM((ROWS, D), BF16),
            pltpu.VMEM((groups, CAP, D), BF16),
            pltpu.VMEM((groups, CAP, D), BF16),
            pltpu.VMEM((PLANES, TP, LANES, FF // TP), BF16),
            pltpu.VMEM((groups, CAP, D), BF16),
            pltpu.VMEM((groups, CAP, D), BF16),
            pltpu.VMEM((TP, D, FF // TP), BF16),
            pltpu.VMEM((TP, D, FF // TP), BF16),
            pltpu.VMEM((TP, FF // TP, D), BF16),
            pltpu.VMEM((PLANES, ROWS, LANES), BF16),
            pltpu.VMEM((PLANES, ROWS, LANES), BF16),
            pltpu.VMEM((ROWS, D), F32),
            pltpu.VMEM((TP, 8, D // TP), F32),
            pltpu.VMEM((TP, ROWS, D // TP), BF16),
            pltpu.VMEM((TP, ROWS, D // TP), BF16),
            dma((3,)), dma((12,)), dma((12,)), dma((3,)), dma((3,)), dma, dma((PLANES,)), dma, dma((PLANES,)),
            dma((4, 3)), dma((4, 3)),
        ],
        compiler_params=pltpu.CompilerParams(
            collective_id=0, has_side_effects=True, vmem_limit_bytes=60 * 1024 * 1024
        ),
    )(
        tokens, norm_gain[None, :], expert_ids.T, group_weight[None, :], expert_logit.T,
        w_gate[0], w_up[0], w_down[0], jnp.broadcast_to(final_gain.astype(F32)[None, :], (8, D // TP)),
    )
    return out.reshape(TP * ROWS, D // TP)


def solution(mesh):
    placed = (
        P(("ep", "tp"), None),
        P(),
        P(("ep", "tp"), None),
        P(("ep", "tp")),
        P(("ep", "tp"), None),
        P("ep", None, "tp"),
        P("ep", None, "tp"),
        P("ep", "tp", None),
        P("tp"),
    )
    return jax.shard_map(
        local, mesh=mesh, in_specs=placed, out_specs=P("ep", "tp"), check_vma=False
    )
```

time: 317 us -> 237 us (0.75); the launches traced: 313 us -> 237 us
  Pallas kernels: 0 us -> 233 us
  waiting for transfers between devices: 221 us -> 0 us
  matrix products: 34.3 us -> 0 us
  starting transfers between devices: 27.9 us -> 0 us
  between operations: 13.6 us -> 0.01 us
  blocking collectives: 9.13 us -> 0 us
  other arithmetic: 5.08 us -> 0 us
    pallas_call x0 -> x1, Pallas kernels: none -> 233 us  [local(): pl.pallas_call(kernel, out_shape=jax.ShapeDtypeStruct((TP, ROWS, D // TP)...]
    all_to_all x3 -> x0, waiting for transfers between devices: 202 us -> none  [the longest x1 94.6 us: local(): lax.all_to_all(product.reshape(experts, CAP, width), 'ep', split_axis=0,...]
    dot_general x7 -> x0, matrix products: 34.3 us -> none  [the longest x1 8.2 us: local(): jnp.dot(hidden, down_whole, preferred_element_type=jnp.float32)]
    all_to_all x3 -> x0, starting transfers between devices: 27.8 us -> none  [the longest x1 13.2 us: local(): lax.all_to_all(outgoing.reshape(experts, CAP, width), 'ep', split_axis=0,...]
    all_gather x2 -> x0, waiting for transfers between devices: 19.1 us -> none  [the longest x1 19.1 us: local(): down_whole = lax.all_gather(w_down, 'tp', axis=1, tiled=True)[0]]
    all_gather x1 -> x0, blocking collectives: 9.13 us -> none  [local(): lax.all_gather(jnp.sum(sliced * sliced, axis=-1), 'tp', axis=0).sum(axis=0)]
  transfers between devices with their start and end apart: 5 -> 0, of which waited for: 4 -> 0; matrix products, arithmetic and copies ran while one was open for 6% -> 0% of each run, Pallas kernels for 0% -> 0%
where the time goes in v2:
time: 237 us
  Pallas kernels  233 us (98%)
  local copies, waits for them, and re-layouts  4.24 us (2%)
    pallas_call x1, Pallas kernels, local(): pl.pallas_call(kernel, out_shape=jax.ShapeDtypeStruct((TP, ROWS, D // TP)...  233 us

profile of v2, /device:TPU:1, one launch (start us, length us, event | category | flops | bytes accessed | tf_op | source)
XLA Modules:
  0.0 237.1 jit_solution(6321529367796985187)
XLA Ops:
  0.0 0.0 copy-start
  0.0 0.7 copy-done
  0.7 0.0 copy-start.1
  0.7 0.6 broadcast_in_dim.12.gain
  1.3 0.1 copy-done.1
  1.4 0.6 broadcast_in_dim.14.final_gain
  2.0 232.9 %shard_map.91 = bf16[4,256,512]{2,1,0:T(8,128)(2,1)} custom-call(bf16[256,2048]{1,0:T(8,128)(2,1)} %tokens.1, bf16[1,2048]{1,0:T(2,128)(2,1)} %broadcast_in_dim.12.gain, s32[2,256]{1,0:T(2,128)} %bitcast.11, f32[1,256]{1,0:T(1,128)} %bitcast.13, f32[2,256]{1,0:T(2,128)} %bitcast.12, bf16[2048,256]{1,0:T(8,128)(2,1)} %bitcast.8, bf16[2048,256]{1,0:T(8,128)(2,1)} %bitcast.9, ...), custom_call_target="tpu_custom_call" | custom-call | tf_op jit(solution)/shard_map/pallas_call | solution.py:289
  234.9 2.3 copy.11
Async XLA Ops:
  0.0 0.7 copy-start
  0.7 0.7 copy-start.1

commit v3 on v1

v3 whole, which is shorter than its diff:
```python
import jax
import jax.numpy as jnp
from jax import lax
from jax.experimental import pallas as pl
from jax.experimental.pallas import tpu as pltpu
from jax.sharding import PartitionSpec as P

D = 2048
FF = 1024
CAP = 16
ROWS = 256
PLANES = 8
GROUP = 8
LANES = GROUP * CAP
TP = 4
COL = D // TP
EPS = 1e-06
MESH = pl.DeviceIdType.MESH
F32 = jnp.float32
BF16 = jnp.bfloat16

A, B, C, DD, E = 0, 20, 40, 48, 56
BLOCK_A, BLOCK_B, BLOCK_C, BLOCK_D, BLOCK_E = range(5)
AT_E, AT_C, AT_D, AT_A, AT_B, AT_UP, AT_DOWN, AT_FAR = range(8)
LANE = (0, 384, 768, 896, 1024)


def kernel(
    tokens, gain, ids, group_weight, logit, w_gate, w_up, w_down, final_gain, out,
    normed, raw, info, pick, packed, routed, hidden, product, returned, wg, wu, wd, high, low,
    far, far_in, near, near_in, residual, slices, squares, inverse_out, inverses,
    own_sem, w_send, w_recv, d_send, d_recv, info_send, info_recv, raw_send, raw_recv, disp_send, disp_recv,
    ret_send, ret_recv, far_send, far_recv, near_send, near_recv, slice_send, slice_recv, inv_send, inv_recv,
):
    ep, tp = lax.axis_index("ep"), lax.axis_index("tp")
    z, inner = ep // GROUP, ep % GROUP
    up1, down1, up2, down2 = ((z + k) % PLANES for k in (1, 7, 2, 6))
    right, left, opposite = (tp + 1) % TP, (tp + 3) % TP, (tp + 2) % TP

    def remote(src, dst, send, recv, to_z, to_inner, to_tp):
        return pltpu.make_async_remote_copy(
            src_ref=src, dst_ref=dst, send_sem=send, recv_sem=recv,
            device_id={"ep": to_z * GROUP + to_inner, "tp": to_tp}, device_id_type=MESH,
        )

    def landed(dst, recv):
        remote(dst, dst, info_send.at[0], recv, z, inner, right).wait_recv()

    def sent(src, send):
        remote(src, src, send, info_recv.at[0], z, inner, right).wait_send()

    barrier = pltpu.get_barrier_semaphore()

    def greet(to_z, to_inner, to_tp):
        pl.semaphore_signal(
            barrier, inc=1, device_id={"ep": to_z * GROUP + to_inner, "tp": to_tp}, device_id_type=MESH
        )

    def greet_plane(i, _):
        o = i // GROUP
        greet((z + PLANES + (1 - 2 * (o % 2)) * (1 + o // 2)) % PLANES, i % GROUP, tp)
        return 0

    def greet_own(j, _):
        greet(z, (inner + j) % GROUP, tp)
        return 0

    lax.fori_loop(0, 4 * GROUP, greet_plane, 0)
    lax.fori_loop(1, GROUP, greet_own, 0)
    for other in (right, left, opposite):
        greet(z, inner, other)

    own = [
        pltpu.make_async_copy(w_gate, wg.at[tp], own_sem.at[0]),
        pltpu.make_async_copy(w_up, wu.at[tp], own_sem.at[1]),
    ] + [
        pltpu.make_async_copy(w_down.at[:, pl.ds(n * COL, COL)], wd.at[tp, n], own_sem.at[2 + n]) for n in range(TP)
    ]
    for copy in own:
        copy.start()

    def norm_rows(i, _):
        at = pl.ds(pl.multiple_of(i * 32, 32), 32)
        t = tokens[at, :].astype(F32)
        inverse = lax.rsqrt(jnp.mean(t * t, axis=-1, keepdims=True) + EPS)
        t = (t * inverse * gain[...].astype(F32)).astype(BF16)
        for n in range(TP):
            normed[n, at, :] = t[:, n * COL:(n + 1) * COL]
        return 0

    lax.fori_loop(0, ROWS // 32, norm_rows, 0)

    id0, id1 = ids[0:1, :], ids[1:2, :]
    lane = lax.broadcasted_iota(jnp.int32, (PLANES * GROUP, ROWS), 0)
    first, second = lane == id0, lane == id1
    named = jnp.where(first, 1.0, jnp.where(second, 1.0, 0.0)).astype(BF16)
    earlier = jnp.where(
        lax.broadcasted_iota(jnp.int32, (ROWS, ROWS), 0)
        < lax.broadcasted_iota(jnp.int32, (ROWS, ROWS), 1), 1.0, 0.0,
    ).astype(BF16)
    before = jnp.dot(named, earlier, preferred_element_type=F32)
    e0, e1 = jnp.exp(logit[0:1, :]), jnp.exp(logit[1:2, :])
    total = e0 + e1
    info[BLOCK_E, 0:1, :] = id0.astype(F32) * CAP + jnp.sum(jnp.where(first, before, 0.0), axis=0, keepdims=True)
    info[BLOCK_E, 1:2, :] = id1.astype(F32) * CAP + jnp.sum(jnp.where(second, before, 0.0), axis=0, keepdims=True)
    info[BLOCK_E, 2:3, :] = group_weight[...] * (e0 / total)
    info[BLOCK_E, 3:4, :] = group_weight[...] * (e1 / total)
    info[BLOCK_E, 4:8, :] = jnp.zeros((4, ROWS), F32)

    sections = {
        BLOCK_A: ((0, 128, z * LANES), (128, 128, up1 * LANES), (256, 64, up2 * LANES)),
        BLOCK_B: ((0, 128, z * LANES), (128, 128, down1 * LANES), (256, 64, down2 * LANES + 64)),
        BLOCK_C: ((0, 128, z * LANES),),
        BLOCK_D: ((0, 128, z * LANES),),
        BLOCK_E: ((0, 128, z * LANES),),
    }
    first_group = {BLOCK_A: A, BLOCK_B: B, BLOCK_C: C, BLOCK_D: DD, BLOCK_E: E}

    def make_pick(block):
        at0, at1 = info[block, 0:1, :], info[block, 1:2, :]
        for start, count, number in sections[block]:
            slot = (lax.broadcasted_iota(jnp.int32, (count, ROWS), 0) + number).astype(F32)
            row = first_group[block] * CAP + start
            pick[row:row + count, :] = jnp.where(slot == at0, 1.0, jnp.where(slot == at1, 1.0, 0.0)).astype(BF16)

    def make_weights(block):
        at0, at1, w0, w1 = (info[block, k:k + 1, :] for k in range(4))
        for start, count, number in sections[block]:
            slot = (lax.broadcasted_iota(jnp.int32, (128, ROWS), 0) + number).astype(F32)
            w = (jnp.where(slot == at0, w0, 0.0) + jnp.where(slot == at1, w1, 0.0)).T[:, :count]
            top_term = w.astype(BF16)
            lanes = slice(LANE[block] + start, LANE[block] + start + count)
            high[:, lanes] = top_term
            low[:, lanes] = (w - top_term.astype(F32)).astype(BF16)

    def pack(block, groups, src, n):
        row = first_group[block] * CAP
        rows = jnp.dot(pick[row:row + groups * CAP, :], src, preferred_element_type=F32).astype(BF16)
        packed[pl.ds(first_group[block], groups), :, pl.ds(pl.multiple_of(n * COL, COL), COL)] = rows.reshape(
            groups, CAP, COL
        )

    def send_own_plane(block, at):
        base = first_group[block]

        def send(j, _):
            to = (inner + j) % GROUP
            remote(packed.at[base + to], routed.at[at * GROUP + inner], disp_send, disp_recv.at[at], z, to, tp).start()
            return 0

        lax.fori_loop(1, GROUP, send, 0)
        routed[at * GROUP + inner] = packed[base + inner]

    make_pick(BLOCK_E)
    for copy in own:
        copy.wait()
    pl.semaphore_wait(barrier, 42)

    def hop_out(n, _):
        remote(normed.at[n], raw.at[0, n], raw_send, raw_recv.at[0, n], up1, inner, tp).start()
        remote(normed.at[n], raw.at[1, n], raw_send, raw_recv.at[1, n], down1, inner, tp).start()
        return 0

    tells = [
        remote(info.at[BLOCK_E], info.at[block], info_send.at[block], info_recv.at[block], to, inner, tp)
        for block, to in ((BLOCK_C, up1), (BLOCK_D, down1), (BLOCK_A, up2), (BLOCK_B, down2))
    ]
    for copy in tells:
        copy.start()
    lax.fori_loop(0, TP, hop_out, 0)

    def weights(src, dst, k, to):
        copy = remote(src, dst, w_send.at[k], w_recv.at[k], z, inner, to)
        copy.start()
        return copy

    flights = [
        weights(wg.at[tp], wg.at[tp], 0, right),
        weights(wu.at[tp], wu.at[tp], 1, left),
        weights(wu.at[tp], wu.at[tp], 2, right),
        weights(wg.at[tp], wg.at[tp], 3, left),
    ]

    def pack_own(n, _):
        pack(BLOCK_E, 8, normed[n], n)
        return 0

    lax.fori_loop(0, TP, pack_own, 0)
    send_own_plane(BLOCK_E, AT_E)
    for copy in tells:
        copy.wait_recv()
    for block in (BLOCK_C, BLOCK_D, BLOCK_A, BLOCK_B):
        make_pick(block)

    def hop_on(n, _):
        landed(raw.at[0, n], raw_recv.at[0, n])
        remote(raw.at[0, n], raw.at[2, n], raw_send, raw_recv.at[2, n], up1, inner, tp).start()
        landed(raw.at[1, n], raw_recv.at[1, n])
        remote(raw.at[1, n], raw.at[3, n], raw_send, raw_recv.at[3, n], down1, inner, tp).start()
        pack(BLOCK_C, 8, raw[0, n], n)
        pack(BLOCK_D, 8, raw[1, n], n)
        return 0

    lax.fori_loop(0, TP, hop_on, 0)
    send_own_plane(BLOCK_C, AT_C)
    send_own_plane(BLOCK_D, AT_D)

    half = FF // TP // 2
    top, bottom = pl.ds(0, half), pl.ds(half, half)

    def down_out(n):
        return [
            remote(wd.at[tp, n], wd.at[tp, n], d_send.at[n, 0], d_recv.at[n, 0], z, inner, right),
            remote(wd.at[tp, n], wd.at[tp, n], d_send.at[n, 1], d_recv.at[n, 1], z, inner, left),
        ]

    def down_on(n):
        return [
            remote(wd.at[left, n, top], wd.at[left, n, top], d_send.at[n, 2], d_recv.at[n, 2], z, inner, right),
            remote(wd.at[right, n, bottom], wd.at[right, n, bottom], d_send.at[n, 3], d_recv.at[n, 3], z, inner, left),
        ]

    def start(copies):
        for copy in copies:
            copy.start()

    flights[0].wait_recv()
    flights.append(weights(wg.at[left], wg.at[left], 4, right))
    flights[1].wait_recv()
    flights.append(weights(wu.at[right], wu.at[right], 5, left))
    outs, ons = [down_out(n) for n in range(TP)], [down_on(n) for n in range(TP)]
    start(outs[0])
    start(outs[1])

    def relay_down(n):
        for copy in outs[n]:
            copy.wait_recv()
        start(ons[n])
        if n + 2 < TP:
            start(outs[n + 2])

    def hop_last(n, _):
        landed(raw.at[2, n], raw_recv.at[2, n])
        landed(raw.at[3, n], raw_recv.at[3, n])
        pack(BLOCK_A, 20, raw[2, n], n)
        pack(BLOCK_B, 20, raw[3, n], n)
        cols = pl.ds(pl.multiple_of(n * COL, COL), COL)

        def send_next(i, _):
            remote(
                packed.at[A + 8 + i, :, cols], routed.at[AT_UP * GROUP + inner, :, cols], disp_send,
                disp_recv.at[AT_UP], up1, i, tp,
            ).start()
            remote(
                packed.at[B + 8 + i, :, cols], routed.at[AT_DOWN * GROUP + inner, :, cols], disp_send,
                disp_recv.at[AT_DOWN], down1, i, tp,
            ).start()
            return 0

        def send_far(i, _):
            remote(
                packed.at[A + 16 + i, :, cols], routed.at[AT_FAR * GROUP + inner, :, cols], disp_send,
                disp_recv.at[AT_FAR], up2, i, tp,
            ).start()
            remote(
                packed.at[B + 16 + i, :, cols], routed.at[AT_FAR * GROUP + inner, :, cols], disp_send,
                disp_recv.at[AT_FAR], down2, 4 + i, tp,
            ).start()
            return 0

        lax.fori_loop(0, 4, send_far, 0)
        lax.fori_loop(0, GROUP, send_next, 0)
        return 0

    lax.fori_loop(0, TP, hop_last, 0)
    send_own_plane(BLOCK_A, AT_A)
    send_own_plane(BLOCK_B, AT_B)

    for block in range(5):
        make_weights(block)

    def expand(q, first_row, count):
        groups = count // CAP
        xs = routed[pl.ds(first_row // CAP, groups)].reshape(count, D)
        g = jnp.dot(xs, wg[q], preferred_element_type=F32)
        u = jnp.dot(xs, wu[q], preferred_element_type=F32)
        hidden[q, pl.ds(first_row, count), :] = (g / (1.0 + jnp.exp(-g)) * u).astype(BF16)

    def expand_near(q):
        def part(i, _):
            expand(q, pl.multiple_of(i * 320, 320), 320)
            return 0

        lax.fori_loop(0, 2, part, 0)

    def expand_all(first_row, count):
        def part(q, _):
            expand(q, first_row, count)
            return 0

        lax.fori_loop(0, TP, part, 0)

    def rows_landed(at, groups):
        landed(routed.at[pl.ds(0, groups)], disp_recv.at[at])

    for at in (AT_E, AT_C, AT_D, AT_A, AT_B):
        rows_landed(at, GROUP - 1)
    expand_near(tp)
    flights[2].wait_recv()
    flights[3].wait_recv()
    expand_near(left)
    expand_near(right)
    flights[4].wait_recv()
    flights[5].wait_recv()
    expand_near(opposite)
    relay_down(0)
    rows_landed(AT_UP, GROUP)
    rows_landed(AT_DOWN, GROUP)
    expand_all(640, 256)
    relay_down(1)
    rows_landed(AT_FAR, GROUP)
    expand_all(896, 128)

    some = (tp + 3) // 4

    def columns_at(k):
        if k < 3:
            return k + some * ((4 + k - tp) // 4)
        return tp + (1 - some) * 3

    upper = inner // 4

    def contract(k):
        n = columns_at(k)
        landed(wd.at[opposite, 0, top], d_recv.at[n, 2])
        landed(wd.at[opposite, 0, bottom], d_recv.at[n, 3])

        def part(i, _):
            at = pl.ds(pl.multiple_of(i * 256, 256), 256)
            rows = jnp.dot(hidden[0, at, :], wd[0, n], preferred_element_type=F32)
            for q in range(1, TP):
                rows += jnp.dot(hidden[q, at, :], wd[q, n], preferred_element_type=F32)
            product[k, pl.ds(i * 16, 16)] = rows.astype(BF16).reshape(16, CAP, COL)
            return 0

        lax.fori_loop(0, 4, part, 0)

        def answer(at, group, block, to_z, i):
            remote(
                product.at[k, at * GROUP + i], returned.at[k, group], ret_send, ret_recv.at[block, k], to_z, i, tp
            ).start()

        def send_far(i, _):
            answer(AT_FAR, 16 + inner + 16 * upper, upper, (z + 6 + 4 * upper) % PLANES, i)
            answer(AT_UP, A + 8 + inner, BLOCK_A, down1, i)
            answer(AT_DOWN, B + 8 + inner, BLOCK_B, up1, i)
            return 0

        ways = ((AT_A, BLOCK_A), (AT_B, BLOCK_B), (AT_C, BLOCK_C), (AT_D, BLOCK_D), (AT_E, BLOCK_E))

        def send_own(j, _):
            to = (inner + j) % GROUP
            for at, block in ways:
                answer(at, first_group[block] + inner, block, z, to)
            return 0

        lax.fori_loop(0, GROUP, send_far, 0)
        lax.fori_loop(1, GROUP, send_own, 0)
        for at, block in ways:
            returned[k, first_group[block] + inner] = product[k, at * GROUP + inner]

    def weighed(block, groups, k):
        remotes = groups - 1
        landed(returned.at[k, pl.ds(0, remotes)], ret_recv.at[block, k])
        rows = returned[k, pl.ds(first_group[block], groups)].reshape(groups * CAP, COL)
        lanes = slice(LANE[block], LANE[block] + groups * CAP)
        return jnp.dot(high[:, lanes], rows, preferred_element_type=F32) + jnp.dot(
            low[:, lanes], rows, preferred_element_type=F32
        )

    def send_partials(k):
        far[0, k] = weighed(BLOCK_A, 20, k).astype(BF16)
        remote(far.at[0, k], far_in.at[0, k], far_send, far_recv.at[0, k], down1, inner, tp).start()
        far[1, k] = weighed(BLOCK_B, 20, k).astype(BF16)
        remote(far.at[1, k], far_in.at[1, k], far_send, far_recv.at[1, k], up1, inner, tp).start()

    def add_partials(k):
        for side, block, to in ((0, BLOCK_C, down1), (1, BLOCK_D, up1)):
            here = weighed(block, 8, k)
            landed(far_in.at[side, k], far_recv.at[side, k])
            near[side, k] = (here + far_in[side, k].astype(F32)).astype(BF16)
            remote(near.at[side, k], near_in.at[side, k], near_send, near_recv.at[side, k], to, inner, tp).start()

    def close(k):
        n = columns_at(k)
        here = weighed(BLOCK_E, 8, k)
        landed(near_in.at[0, k], near_recv.at[0, k])
        landed(near_in.at[1, k], near_recv.at[1, k])
        t = tokens[:, pl.ds(pl.multiple_of(n * COL, COL), COL)].astype(F32)
        r = (t + here + near_in[0, k].astype(F32) + near_in[1, k].astype(F32)).astype(BF16)
        residual[k] = r
        s = r.astype(F32)
        s = s * s
        s = s[:, 0:128] + s[:, 128:256] + s[:, 256:384] + s[:, 384:512]
        squares[...] = s if k == 0 else squares[...] + s

        @pl.when(n != tp)
        def _():
            remote(residual.at[k], slices.at[tp], slice_send, slice_recv.at[tp], z, inner, n).start()

        @pl.when(n == tp)
        def _():
            slices[tp] = residual[k]

    contract(0)
    relay_down(2)
    contract(1)
    send_partials(0)
    relay_down(3)
    contract(2)
    send_partials(1)
    add_partials(0)
    contract(3)
    send_partials(2)
    add_partials(1)
    close(0)
    send_partials(3)
    add_partials(2)
    close(1)
    add_partials(3)
    close(2)
    close(3)

    inverse = lax.rsqrt(jnp.sum(squares[...], axis=-1, keepdims=True) / D + EPS)
    inverse_out[...] = jnp.broadcast_to(inverse, (ROWS, 128)).T[0:8, :]
    lasts = [
        remote(inverse_out, inverses.at[tp], inv_send.at[k], inv_recv.at[k], z, inner, other)
        for k, other in enumerate((right, left, opposite))
    ]
    start(lasts)
    inverses[tp] = inverse_out[...]

    def finish(source):
        column = jnp.broadcast_to(inverses[source, 0:1, :], (128, ROWS)).T[:, 0:1]
        out[source] = (slices[source].astype(F32) * column * final_gain[...]).astype(BF16)

    finish(tp)
    for copy in lasts:
        copy.wait_recv()
    for other in (right, left, opposite):
        landed(slices.at[other], slice_recv.at[other])
        finish(other)

    for copy in tells + flights + lasts + sum(outs, []) + sum(ons, []):
        copy.wait_send()
    sent(raw, raw_send)
    sent(routed.at[pl.ds(0, 59)], disp_send)
    sent(routed.at[pl.ds(0, 59)], ret_send)
    sent(far, far_send)
    sent(near, near_send)
    sent(slices.at[pl.ds(0, 3)], slice_send)


def local(
    tokens, norm_gain, expert_ids, group_weight, expert_logit, w_gate, w_up, w_down, final_gain
):
    vmem = pl.BlockSpec(memory_space=pltpu.VMEM)
    anywhere = pl.BlockSpec(memory_space=pl.ANY)
    dma, groups = pltpu.SemaphoreType.DMA, PLANES * GROUP
    out = pl.pallas_call(
        kernel,
        out_shape=jax.ShapeDtypeStruct((TP, ROWS, COL), BF16),
        in_specs=[vmem] * 5 + [anywhere] * 3 + [vmem],
        out_specs=vmem,
        scratch_shapes=[
            pltpu.VMEM((TP, ROWS, COL), BF16),
            pltpu.VMEM((4, TP, ROWS, COL), BF16),
            pltpu.VMEM((5, 8, ROWS), F32),
            pltpu.VMEM((groups * CAP, ROWS), BF16),
            pltpu.VMEM((groups, CAP, D), BF16),
            pltpu.VMEM((groups, CAP, D), BF16),
            pltpu.VMEM((TP, groups * CAP, FF // TP), BF16),
            pltpu.VMEM((TP, groups, CAP, COL), BF16),
            pltpu.VMEM((TP, groups, CAP, COL), BF16),
            pltpu.VMEM((TP, D, FF // TP), BF16),
            pltpu.VMEM((TP, D, FF // TP), BF16),
            pltpu.VMEM((TP, TP, FF // TP, COL), BF16),
            pltpu.VMEM((ROWS, 1152), BF16),
            pltpu.VMEM((ROWS, 1152), BF16),
            pltpu.VMEM((2, TP, ROWS, COL), BF16),
            pltpu.VMEM((2, TP, ROWS, COL), BF16),
            pltpu.VMEM((2, TP, ROWS, COL), BF16),
            pltpu.VMEM((2, TP, ROWS, COL), BF16),
            pltpu.VMEM((TP, ROWS, COL), BF16),
            pltpu.VMEM((TP, ROWS, COL), BF16),
            pltpu.VMEM((ROWS, 128), F32),
            pltpu.VMEM((8, ROWS), F32),
            pltpu.VMEM((TP, 8, ROWS), F32),
            dma((6,)), dma((6,)), dma((6,)), dma((TP, 4)), dma((TP, 4)), dma((4,)), dma((4,)), dma, dma((4, TP)),
            dma, dma((PLANES,)), dma, dma((5, TP)), dma, dma((2, TP)), dma, dma((2, TP)), dma, dma((TP,)),
            dma((3,)), dma((3,)),
        ],
        compiler_params=pltpu.CompilerParams(
            collective_id=0, has_side_effects=True, vmem_limit_bytes=62 * 1024 * 1024
        ),
    )(
        tokens, norm_gain[None, :], expert_ids.T, group_weight[None, :], expert_logit.T,
        w_gate[0], w_up[0], w_down[0], final_gain.astype(F32)[None, :],
    )
    return out.reshape(TP * ROWS, COL)


def solution(mesh):
    placed = (
        P(("ep", "tp"), None),
        P(),
        P(("ep", "tp"), None),
        P(("ep", "tp")),
        P(("ep", "tp"), None),
        P("ep", None, "tp"),
        P("ep", None, "tp"),
        P("ep", "tp", None),
        P("tp"),
    )
    return jax.shard_map(
        local, mesh=mesh, in_specs=placed, out_specs=P("ep", "tp"), check_vma=False
    )
```

time: 317 us -> 204 us (0.64); the launches traced: 313 us -> 203 us
  waiting for transfers between devices: 221 us -> 0 us
  Pallas kernels: 0 us -> 199 us
  matrix products: 34.3 us -> 0 us
  starting transfers between devices: 27.9 us -> 0 us
  between operations: 13.6 us -> 0.01 us
  blocking collectives: 9.13 us -> 0 us
  other arithmetic: 5.08 us -> 0.56 us
    all_to_all x3 -> x0, waiting for transfers between devices: 202 us -> none  [the longest x1 94.6 us: local(): lax.all_to_all(product.reshape(experts, CAP, width), 'ep', split_axis=0,...]
    pallas_call x0 -> x1, Pallas kernels: none -> 199 us  [local(): pl.pallas_call(kernel, out_shape=jax.ShapeDtypeStruct((TP, ROWS, COL), BF...]
    dot_general x7 -> x0, matrix products: 34.3 us -> none  [the longest x1 8.2 us: local(): jnp.dot(hidden, down_whole, preferred_element_type=jnp.float32)]
    all_to_all x3 -> x0, starting transfers between devices: 27.8 us -> none  [the longest x1 13.2 us: local(): lax.all_to_all(outgoing.reshape(experts, CAP, width), 'ep', split_axis=0,...]
    all_gather x2 -> x0, waiting for transfers between devices: 19.1 us -> none  [the longest x1 19.1 us: local(): down_whole = lax.all_gather(w_down, 'tp', axis=1, tiled=True)[0]]
    all_gather x1 -> x0, blocking collectives: 9.13 us -> none  [local(): lax.all_gather(jnp.sum(sliced * sliced, axis=-1), 'tp', axis=0).sum(axis=0)]
  transfers between devices with their start and end apart: 5 -> 0, of which waited for: 4 -> 0; matrix products, arithmetic and copies ran while one was open for 6% -> 0% of each run, Pallas kernels for 0% -> 0%
where the time goes in v3:
time: 204 us; the launch traced here: 203 us
  Pallas kernels  199 us (98%)
  local copies, waits for them, and re-layouts  3.55 us (2%)
    pallas_call x1, Pallas kernels, local(): pl.pallas_call(kernel, out_shape=jax.ShapeDtypeStruct((TP, ROWS, COL), BF...  199 us

profile of v3, /device:TPU:1, one launch (start us, length us, event | category | flops | bytes accessed | tf_op | source)
XLA Modules:
  0.0 203.0 jit_solution(14468084425363394278)
XLA Ops:
  0.0 0.0 copy-start.1
  0.0 0.0 copy-start
  0.0 0.7 copy-done.1
  0.7 0.6 broadcast_in_dim.15
  1.2 0.0 copy-done
  1.2 0.6 broadcast_in_dim.11.gain
  1.9 198.9 %shard_map.91 = bf16[4,256,512]{2,1,0:T(8,128)(2,1)} custom-call(bf16[256,2048]{1,0:T(8,128)(2,1)} %tokens.1, bf16[1,2048]{1,0:T(2,128)(2,1)} %broadcast_in_dim.11.gain, s32[2,256]{1,0:T(2,128)} %bitcast.13, f32[1,256]{1,0:T(1,128)} %bitcast.15, f32[2,256]{1,0:T(2,128)} %bitcast.14, bf16[2048,256]{1,0:T(8,128)(2,1)} %bitcast.9, bf16[2048,256]{1,0:T(8,128)(2,1)} %bitcast.10, ...), custom_call_target="tpu_custom_call" | custom-call | tf_op jit(solution)/shard_map/pallas_call | solution.py:470
  200.7 2.3 %copy.11 = bf16[1024,512]{1,0:T(8,128)(2,1)} copy(bf16[1024,512]{1,0:T(8,128)(2,1)} %bitcast.8) | data formatting | bytes 2097152
Async XLA Ops:
  0.0 0.7 copy-start.1
  0.0 1.2 copy-start

commit v4 on v3

--- a/solution.py
+++ b/solution.py
@@ -83,7 +83,7 @@
         at = pl.ds(pl.multiple_of(i * 32, 32), 32)
         t = tokens[at, :].astype(F32)
         inverse = lax.rsqrt(jnp.mean(t * t, axis=-1, keepdims=True) + EPS)
-        t = (t * inverse * gain[...].astype(F32)).astype(BF16)
+        t = (t * inverse * gain[...].astype(F32)[None, :]).astype(BF16)
         for n in range(TP):
             normed[n, at, :] = t[:, n * COL:(n + 1) * COL]
         return 0
@@ -140,16 +140,21 @@
             groups, CAP, COL
         )
 
-    def send_own_plane(block, at):
-        base = first_group[block]
+    def send_own_plane(ways, n):
+        cols = pl.ds(pl.multiple_of(n * COL, COL), COL)
 
         def send(j, _):
             to = (inner + j) % GROUP
-            remote(packed.at[base + to], routed.at[at * GROUP + inner], disp_send, disp_recv.at[at], z, to, tp).start()
+            for block, at in ways:
+                remote(
+                    packed.at[first_group[block] + to, :, cols], routed.at[at * GROUP + inner, :, cols], disp_send,
+                    disp_recv.at[at], z, to, tp,
+                ).start()
             return 0
 
         lax.fori_loop(1, GROUP, send, 0)
-        routed[at * GROUP + inner] = packed[base + inner]
+        for block, at in ways:
+            routed[at * GROUP + inner, :, cols] = packed[first_group[block] + inner, :, cols]
 
     make_pick(BLOCK_E)
     for copy in own:
@@ -183,10 +188,10 @@
 
     def pack_own(n, _):
         pack(BLOCK_E, 8, normed[n], n)
+        send_own_plane(((BLOCK_E, AT_E),), n)
         return 0
 
     lax.fori_loop(0, TP, pack_own, 0)
-    send_own_plane(BLOCK_E, AT_E)
     for copy in tells:
         copy.wait_recv()
     for block in (BLOCK_C, BLOCK_D, BLOCK_A, BLOCK_B):
@@ -199,26 +204,25 @@
         remote(raw.at[1, n], raw.at[3, n], raw_send, raw_recv.at[3, n], down1, inner, tp).start()
         pack(BLOCK_C, 8, raw[0, n], n)
         pack(BLOCK_D, 8, raw[1, n], n)
+        send_own_plane(((BLOCK_C, AT_C), (BLOCK_D, AT_D)), n)
         return 0
 
     lax.fori_loop(0, TP, hop_on, 0)
-    send_own_plane(BLOCK_C, AT_C)
-    send_own_plane(BLOCK_D, AT_D)
 
     half = FF // TP // 2
     top, bottom = pl.ds(0, half), pl.ds(half, half)
 
+    def over_y(q, n, part, k, to):
+        return remote(wd.at[q, n, part], wd.at[q, n, part], d_send.at[n, k], d_recv.at[n, k], z, inner, to)
+
     def down_out(n):
         return [
-            remote(wd.at[tp, n], wd.at[tp, n], d_send.at[n, 0], d_recv.at[n, 0], z, inner, right),
-            remote(wd.at[tp, n], wd.at[tp, n], d_send.at[n, 1], d_recv.at[n, 1], z, inner, left),
+            over_y(tp, n, top, 0, right), over_y(tp, n, bottom, 1, left),
+            over_y(tp, n, bottom, 4, right), over_y(tp, n, top, 5, left),
         ]
 
     def down_on(n):
-        return [
-            remote(wd.at[left, n, top], wd.at[left, n, top], d_send.at[n, 2], d_recv.at[n, 2], z, inner, right),
-            remote(wd.at[right, n, bottom], wd.at[right, n, bottom], d_send.at[n, 3], d_recv.at[n, 3], z, inner, left),
-        ]
+        return [over_y(left, n, top, 2, right), over_y(right, n, bottom, 3, left)]
 
     def start(copies):
         for copy in copies:
@@ -228,22 +232,46 @@
     flights.append(weights(wg.at[left], wg.at[left], 4, right))
     flights[1].wait_recv()
     flights.append(weights(wu.at[right], wu.at[right], 5, left))
-    outs, ons = [down_out(n) for n in range(TP)], [down_on(n) for n in range(TP)]
+    outs, ons = [down_out(n) for n in (0, 2, 3, 1)], [down_on(n) for n in (0, 2, 3, 1)]
     start(outs[0])
-    start(outs[1])
-
-    def relay_down(n):
-        for copy in outs[n]:
-            copy.wait_recv()
-        start(ons[n])
-        if n + 2 < TP:
-            start(outs[n + 2])
+
+    def relay_down(k):
+        outs[k][0].wait_recv()
+        outs[k][1].wait_recv()
+        start(ons[k])
+        if k + 1 < TP:
+            start(outs[k + 1])
+
+    def expand(q, first_row, count):
+        groups = count // CAP
+        xs = routed[pl.ds(first_row // CAP, groups)].reshape(count, D)
+        g = jnp.dot(xs, wg[q], preferred_element_type=F32)
+        u = jnp.dot(xs, wu[q], preferred_element_type=F32)
+        hidden[q, pl.ds(first_row, count), :] = (g / (1.0 + jnp.exp(-g)) * u).astype(BF16)
+
+    def expand_of(order, first_row, count):
+        def part(i, _):
+            expand((tp + order[0] + order[1] * i) % TP, first_row, count)
+            return 0
+
+        lax.fori_loop(0, order[2], part, 0)
+
+    def rows_landed(at, groups):
+        landed(routed.at[pl.ds(0, groups)], disp_recv.at[at])
+
+    for block in range(5):
+        make_weights(block)
+    rows_landed(AT_E, GROUP - 1)
+    rows_landed(AT_C, GROUP - 1)
+    rows_landed(AT_D, GROUP - 1)
+    expand_of((0, 0, 1), 0, 384)
 
     def hop_last(n, _):
         landed(raw.at[2, n], raw_recv.at[2, n])
         landed(raw.at[3, n], raw_recv.at[3, n])
         pack(BLOCK_A, 20, raw[2, n], n)
         pack(BLOCK_B, 20, raw[3, n], n)
+        send_own_plane(((BLOCK_A, AT_A), (BLOCK_B, AT_B)), n)
         cols = pl.ds(pl.multiple_of(n * COL, COL), COL)
 
         def send_next(i, _):
@@ -273,67 +301,32 @@
         return 0
 
     lax.fori_loop(0, TP, hop_last, 0)
-    send_own_plane(BLOCK_A, AT_A)
-    send_own_plane(BLOCK_B, AT_B)
-
-    for block in range(5):
-        make_weights(block)
-
-    def expand(q, first_row, count):
-        groups = count // CAP
-        xs = routed[pl.ds(first_row // CAP, groups)].reshape(count, D)
-        g = jnp.dot(xs, wg[q], preferred_element_type=F32)
-        u = jnp.dot(xs, wu[q], preferred_element_type=F32)
-        hidden[q, pl.ds(first_row, count), :] = (g / (1.0 + jnp.exp(-g)) * u).astype(BF16)
-
-    def expand_near(q):
-        def part(i, _):
-            expand(q, pl.multiple_of(i * 320, 320), 320)
-            return 0
-
-        lax.fori_loop(0, 2, part, 0)
-
-    def expand_all(first_row, count):
-        def part(q, _):
-            expand(q, first_row, count)
-            return 0
-
-        lax.fori_loop(0, TP, part, 0)
-
-    def rows_landed(at, groups):
-        landed(routed.at[pl.ds(0, groups)], disp_recv.at[at])
-
-    for at in (AT_E, AT_C, AT_D, AT_A, AT_B):
-        rows_landed(at, GROUP - 1)
-    expand_near(tp)
+
     flights[2].wait_recv()
     flights[3].wait_recv()
-    expand_near(left)
-    expand_near(right)
+    expand_of((1, 2, 2), 0, 384)
+    rows_landed(AT_A, GROUP - 1)
+    rows_landed(AT_B, GROUP - 1)
+    expand_of((3, 1, 3), 384, 256)
     flights[4].wait_recv()
     flights[5].wait_recv()
-    expand_near(opposite)
+    expand_of((2, 0, 1), 0, 640)
     relay_down(0)
     rows_landed(AT_UP, GROUP)
     rows_landed(AT_DOWN, GROUP)
-    expand_all(640, 256)
-    relay_down(1)
     rows_landed(AT_FAR, GROUP)
-    expand_all(896, 128)
-
-    some = (tp + 3) // 4
+    expand_of((0, 1, 4), 640, 384)
 
     def columns_at(k):
-        if k < 3:
-            return k + some * ((4 + k - tp) // 4)
-        return tp + (1 - some) * 3
+        last = tp // 3
+        return (0, 2, 3 - 2 * last, 1 + 2 * last)[k]
 
     upper = inner // 4
 
     def contract(k):
         n = columns_at(k)
-        landed(wd.at[opposite, 0, top], d_recv.at[n, 2])
-        landed(wd.at[opposite, 0, bottom], d_recv.at[n, 3])
+        for sem in range(2, 6):
+            landed(wd.at[opposite, 0, top], d_recv.at[n, sem])
 
         def part(i, _):
             at = pl.ds(pl.multiple_of(i * 256, 256), 256)
@@ -358,14 +351,16 @@
 
         ways = ((AT_A, BLOCK_A), (AT_B, BLOCK_B), (AT_C, BLOCK_C), (AT_D, BLOCK_D), (AT_E, BLOCK_E))
 
-        def send_own(j, _):
-            to = (inner + j) % GROUP
-            for at, block in ways:
-                answer(at, first_group[block] + inner, block, z, to)
-            return 0
-
         lax.fori_loop(0, GROUP, send_far, 0)
-        lax.fori_loop(1, GROUP, send_own, 0)
+        for some in (ways[0:2], ways[2:4], ways[4:5]):
+
+            def send_own(j, _):
+                to = (inner + j) % GROUP
+                for at, block in some:
+                    answer(at, first_group[block] + inner, block, z, to)
+                return 0
+
+            lax.fori_loop(1, GROUP, send_own, 0)
         for at, block in ways:
             returned[k, first_group[block] + inner] = product[k, at * GROUP + inner]
 
@@ -413,8 +408,9 @@
             slices[tp] = residual[k]
 
     contract(0)
+    relay_down(1)
+    contract(1)
     relay_down(2)
-    contract(1)
     send_partials(0)
     relay_down(3)
     contract(2)
@@ -442,7 +438,7 @@
 
     def finish(source):
         column = jnp.broadcast_to(inverses[source, 0:1, :], (128, ROWS)).T[:, 0:1]
-        out[source] = (slices[source].astype(F32) * column * final_gain[...]).astype(BF16)
+        out[source] = (slices[source].astype(F32) * column * final_gain[...].astype(F32)[None, :]).astype(BF16)
 
     finish(tp)
     for copy in lasts:
@@ -496,7 +492,7 @@
             pltpu.VMEM((ROWS, 128), F32),
             pltpu.VMEM((8, ROWS), F32),
             pltpu.VMEM((TP, 8, ROWS), F32),
-            dma((6,)), dma((6,)), dma((6,)), dma((TP, 4)), dma((TP, 4)), dma((4,)), dma((4,)), dma, dma((4, TP)),
+            dma((6,)), dma((6,)), dma((6,)), dma((TP, 6)), dma((TP, 6)), dma((4,)), dma((4,)), dma, dma((4, TP)),
             dma, dma((PLANES,)), dma, dma((5, TP)), dma, dma((2, TP)), dma, dma((2, TP)), dma, dma((TP,)),
             dma((3,)), dma((3,)),
         ],
@@ -504,8 +500,8 @@
             collective_id=0, has_side_effects=True, vmem_limit_bytes=62 * 1024 * 1024
         ),
     )(
-        tokens, norm_gain[None, :], expert_ids.T, group_weight[None, :], expert_logit.T,
-        w_gate[0], w_up[0], w_down[0], final_gain.astype(F32)[None, :],
+        tokens, norm_gain, expert_ids.T, group_weight[None, :], expert_logit.T,
+        w_gate[0], w_up[0], w_down[0], final_gain,
     )
     return out.reshape(TP * ROWS, COL)
 

time: 204 us -> 185 us (0.907)
  the two profiles are of different devices: /device:TPU:1 before, /device:TPU:8 now
where the time goes in v4:
time: 185 us
  Pallas kernels  183 us (99%)
  local copies, waits for them, and re-layouts  2.26 us (1%)
    pallas_call x1, Pallas kernels, local(): pl.pallas_call(kernel, out_shape=jax.ShapeDtypeStruct((TP, ROWS, COL), BF...  183 us

profile of v4, /device:TPU:8, one launch (start us, length us, event | category | flops | bytes accessed | tf_op | source)
XLA Modules:
  0.0 185.3 jit_solution(3470071317780656674)
XLA Ops:
  0.0 183.0 %shard_map.91 = bf16[4,256,512]{2,1,0:T(8,128)(2,1)} custom-call(bf16[256,2048]{1,0:T(8,128)(2,1)} %tokens.1, bf16[2048]{0:T(1024)(128)(2,1)} %gain.1, s32[2,256]{1,0:T(2,128)} %bitcast.11, f32[1,256]{1,0:T(1,128)} %bitcast.13, f32[2,256]{1,0:T(2,128)} %bitcast.12, bf16[2048,256]{1,0:T(8,128)(2,1)} %bitcast.8, bf16[2048,256]{1,0:T(8,128)(2,1)} %bitcast.9, ...), custom_call_target="tpu_custom_call" | custom-call | tf_op jit(solution)/shard_map/pallas_call | solution.py:466
  183.0 2.3 %copy.11 = bf16[1024,512]{1,0:T(8,128)(2,1)} copy(bf16[1024,512]{1,0:T(8,128)(2,1)} %bitcast.7) | data formatting | bytes 2097152

commit v5 on v4

--- a/solution.py
+++ b/solution.py
@@ -14,6 +14,8 @@
 LANES = GROUP * CAP
 TP = 4
 COL = D // TP
+HALF = COL // 2
+STAGES = 2 * TP
 EPS = 1e-06
 MESH = pl.DeviceIdType.MESH
 F32 = jnp.float32
@@ -26,10 +28,11 @@
 
 
 def kernel(
-    tokens, gain, ids, group_weight, logit, w_gate, w_up, w_down, final_gain, out,
+    tokens_in, gain_in, ids_in, group_weight_in, logit_in, w_gate, w_up, w_down, final_gain_in, out,
+    tokens, gain, ids, group_weight, logit, final_gain, done,
     normed, raw, info, pick, packed, routed, hidden, product, returned, wg, wu, wd, high, low,
     far, far_in, near, near_in, residual, slices, squares, inverse_out, inverses,
-    own_sem, w_send, w_recv, d_send, d_recv, info_send, info_recv, raw_send, raw_recv, disp_send, disp_recv,
+    in_sem, done_sem, own_sem, w_send, w_recv, d_send, d_recv, info_send, info_recv, raw_send, raw_recv, disp_send, disp_recv,
     ret_send, ret_recv, far_send, far_recv, near_send, near_recv, slice_send, slice_recv, inv_send, inv_recv,
 ):
     ep, tp = lax.axis_index("ep"), lax.axis_index("tp")
@@ -58,7 +61,7 @@
 
     def greet_plane(i, _):
         o = i // GROUP
-        greet((z + PLANES + (1 - 2 * (o % 2)) * (1 + o // 2)) % PLANES, i % GROUP, tp)
+        greet((z + PLANES + (1 - 2 * (o % 2)) * (2 - o // 2)) % PLANES, i % GROUP, tp)
         return 0
 
     def greet_own(j, _):
@@ -70,12 +73,23 @@
     for other in (right, left, opposite):
         greet(z, inner, other)
 
+    inputs = [
+        pltpu.make_async_copy(src, dst, in_sem.at[k])
+        for k, (src, dst) in enumerate((
+            (tokens_in, tokens), (gain_in, gain), (ids_in, ids), (group_weight_in, group_weight),
+            (logit_in, logit), (final_gain_in, final_gain),
+        ))
+    ]
+    for copy in inputs:
+        copy.start()
     own = [
         pltpu.make_async_copy(w_gate, wg.at[tp], own_sem.at[0]),
         pltpu.make_async_copy(w_up, wu.at[tp], own_sem.at[1]),
     ] + [
         pltpu.make_async_copy(w_down.at[:, pl.ds(n * COL, COL)], wd.at[tp, n], own_sem.at[2 + n]) for n in range(TP)
     ]
+    for copy in inputs:
+        copy.wait()
     for copy in own:
         copy.start()
 
@@ -89,6 +103,22 @@
         return 0
 
     lax.fori_loop(0, ROWS // 32, norm_rows, 0)
+
+    for copy in own:
+        copy.wait()
+    pl.semaphore_wait(barrier, 42)
+
+    def weights(src, dst, k, to):
+        copy = remote(src, dst, w_send.at[k], w_recv.at[k], z, inner, to)
+        copy.start()
+        return copy
+
+    flights = [
+        weights(wg.at[tp], wg.at[tp], 0, right),
+        weights(wu.at[tp], wu.at[tp], 1, left),
+        weights(wu.at[tp], wu.at[tp], 2, right),
+        weights(wg.at[tp], wg.at[tp], 3, left),
+    ]
 
     id0, id1 = ids[0:1, :], ids[1:2, :]
     lane = lax.broadcasted_iota(jnp.int32, (PLANES * GROUP, ROWS), 0)
@@ -108,25 +138,30 @@
     info[BLOCK_E, 4:8, :] = jnp.zeros((4, ROWS), F32)
 
     sections = {
-        BLOCK_A: ((0, 128, z * LANES), (128, 128, up1 * LANES), (256, 64, up2 * LANES)),
-        BLOCK_B: ((0, 128, z * LANES), (128, 128, down1 * LANES), (256, 64, down2 * LANES + 64)),
-        BLOCK_C: ((0, 128, z * LANES),),
-        BLOCK_D: ((0, 128, z * LANES),),
-        BLOCK_E: ((0, 128, z * LANES),),
+        BLOCK_A: ((0, 128, z * LANES, 1), (128, 128, up1 * LANES, 1), (256, 64, up2 * LANES, 2)),
+        BLOCK_B: ((0, 128, z * LANES, 1), (128, 128, down1 * LANES, 1), (256, 64, down2 * LANES + CAP, 2)),
+        BLOCK_C: ((0, 128, z * LANES, 1),),
+        BLOCK_D: ((0, 128, z * LANES, 1),),
+        BLOCK_E: ((0, 128, z * LANES, 1),),
     }
+
+    def slots(count, number, step):
+        row = lax.broadcasted_iota(jnp.int32, (count, ROWS), 0)
+        return (row + (step - 1) * CAP * lax.div(row, CAP) + number).astype(F32)
+
     first_group = {BLOCK_A: A, BLOCK_B: B, BLOCK_C: C, BLOCK_D: DD, BLOCK_E: E}
 
     def make_pick(block):
         at0, at1 = info[block, 0:1, :], info[block, 1:2, :]
-        for start, count, number in sections[block]:
-            slot = (lax.broadcasted_iota(jnp.int32, (count, ROWS), 0) + number).astype(F32)
+        for start, count, number, step in sections[block]:
+            slot = slots(count, number, step)
             row = first_group[block] * CAP + start
             pick[row:row + count, :] = jnp.where(slot == at0, 1.0, jnp.where(slot == at1, 1.0, 0.0)).astype(BF16)
 
     def make_weights(block):
         at0, at1, w0, w1 = (info[block, k:k + 1, :] for k in range(4))
-        for start, count, number in sections[block]:
-            slot = (lax.broadcasted_iota(jnp.int32, (128, ROWS), 0) + number).astype(F32)
+        for start, count, number, step in sections[block]:
+            slot = slots(128, number, step)
             w = (jnp.where(slot == at0, w0, 0.0) + jnp.where(slot == at1, w1, 0.0)).T[:, :count]
             top_term = w.astype(BF16)
             lanes = slice(LANE[block] + start, LANE[block] + start + count)
@@ -156,35 +191,21 @@
         for block, at in ways:
             routed[at * GROUP + inner, :, cols] = packed[first_group[block] + inner, :, cols]
 
-    make_pick(BLOCK_E)
-    for copy in own:
-        copy.wait()
-    pl.semaphore_wait(barrier, 42)
-
-    def hop_out(n, _):
-        remote(normed.at[n], raw.at[0, n], raw_send, raw_recv.at[0, n], up1, inner, tp).start()
-        remote(normed.at[n], raw.at[1, n], raw_send, raw_recv.at[1, n], down1, inner, tp).start()
-        return 0
-
     tells = [
         remote(info.at[BLOCK_E], info.at[block], info_send.at[block], info_recv.at[block], to, inner, tp)
         for block, to in ((BLOCK_C, up1), (BLOCK_D, down1), (BLOCK_A, up2), (BLOCK_B, down2))
     ]
     for copy in tells:
         copy.start()
+
+    def hop_out(n, _):
+        remote(normed.at[n], raw.at[0, n], raw_send, raw_recv.at[0, n], up1, inner, tp).start()
+        remote(normed.at[n], raw.at[1, n], raw_send, raw_recv.at[1, n], down1, inner, tp).start()
+        return 0
+
     lax.fori_loop(0, TP, hop_out, 0)
 
-    def weights(src, dst, k, to):
-        copy = remote(src, dst, w_send.at[k], w_recv.at[k], z, inner, to)
-        copy.start()
-        return copy
-
-    flights = [
-        weights(wg.at[tp], wg.at[tp], 0, right),
-        weights(wu.at[tp], wu.at[tp], 1, left),
-        weights(wu.at[tp], wu.at[tp], 2, right),
-        weights(wg.at[tp], wg.at[tp], 3, left),
-    ]
+    make_pick(BLOCK_E)
 
     def pack_own(n, _):
         pack(BLOCK_E, 8, normed[n], n)
@@ -288,11 +309,11 @@
         def send_far(i, _):
             remote(
                 packed.at[A + 16 + i, :, cols], routed.at[AT_FAR * GROUP + inner, :, cols], disp_send,
-                disp_recv.at[AT_FAR], up2, i, tp,
+                disp_recv.at[AT_FAR], up2, 2 * i, tp,
             ).start()
             remote(
                 packed.at[B + 16 + i, :, cols], routed.at[AT_FAR * GROUP + inner, :, cols], disp_send,
-                disp_recv.at[AT_FAR], down2, 4 + i, tp,
+                disp_recv.at[AT_FAR], down2, 2 * i + 1, tp,
             ).start()
             return 0
 
@@ -317,57 +338,64 @@
     rows_landed(AT_FAR, GROUP)
     expand_of((0, 1, 4), 640, 384)
 
+    last = tp // 3
+
     def columns_at(k):
-        last = tp // 3
-        return (0, 2, 3 - 2 * last, 1 + 2 * last)[k]
-
-    upper = inner // 4
+        if k < 5:
+            return (0, 0, 2, 2, 3)[k], k % 2
+        return (3 - 2 * last, 1, 1 + 2 * last)[k - 5], (1 - last, last, 1)[k - 5]
+
+    odd = inner % 2
+    ways = ((AT_A, BLOCK_A), (AT_B, BLOCK_B), (AT_C, BLOCK_C), (AT_D, BLOCK_D), (AT_E, BLOCK_E))
 
     def contract(k):
-        n = columns_at(k)
-        for sem in range(2, 6):
-            landed(wd.at[opposite, 0, top], d_recv.at[n, sem])
+        n, h = columns_at(k)
+        cols = pl.ds(pl.multiple_of(h * HALF, HALF), HALF)
+        if k in (0, 2, 4, 5):
+            for sem in range(2, 6):
+                landed(wd.at[opposite, 0, top], d_recv.at[(0, 0, 2, 2, 3, 1)[k], sem])
 
         def part(i, _):
             at = pl.ds(pl.multiple_of(i * 256, 256), 256)
-            rows = jnp.dot(hidden[0, at, :], wd[0, n], preferred_element_type=F32)
+            rows = jnp.dot(hidden[0, at, :], wd[0, n, :, cols], preferred_element_type=F32)
             for q in range(1, TP):
-                rows += jnp.dot(hidden[q, at, :], wd[q, n], preferred_element_type=F32)
-            product[k, pl.ds(i * 16, 16)] = rows.astype(BF16).reshape(16, CAP, COL)
+                rows += jnp.dot(hidden[q, at, :], wd[q, n, :, cols], preferred_element_type=F32)
+            product[k, pl.ds(i * 16, 16)] = rows.astype(BF16).reshape(16, CAP, HALF)
             return 0
 
         lax.fori_loop(0, 4, part, 0)
 
-        def answer(at, group, block, to_z, i):
-            remote(
-                product.at[k, at * GROUP + i], returned.at[k, group], ret_send, ret_recv.at[block, k], to_z, i, tp
-            ).start()
-
         def send_far(i, _):
-            answer(AT_FAR, 16 + inner + 16 * upper, upper, (z + 6 + 4 * upper) % PLANES, i)
-            answer(AT_UP, A + 8 + inner, BLOCK_A, down1, i)
-            answer(AT_DOWN, B + 8 + inner, BLOCK_B, up1, i)
-            return 0
-
-        ways = ((AT_A, BLOCK_A), (AT_B, BLOCK_B), (AT_C, BLOCK_C), (AT_D, BLOCK_D), (AT_E, BLOCK_E))
+            answer(k, AT_FAR, A + 16 + inner // 2 + (B - A) * odd, odd, (z + 6 + 4 * odd) % PLANES, i)
+            answer(k, AT_UP, A + 8 + inner, BLOCK_A, down1, i)
+            answer(k, AT_DOWN, B + 8 + inner, BLOCK_B, up1, i)
+            return 0
 
         lax.fori_loop(0, GROUP, send_far, 0)
-        for some in (ways[0:2], ways[2:4], ways[4:5]):
-
-            def send_own(j, _):
-                to = (inner + j) % GROUP
-                for at, block in some:
-                    answer(at, first_group[block] + inner, block, z, to)
-                return 0
-
-            lax.fori_loop(1, GROUP, send_own, 0)
-        for at, block in ways:
+        answer_plane(k, ways[0:2])
+
+    def answer(k, at, group, block, to_z, i):
+        remote(product.at[k, at * GROUP + i], returned.at[k, group], ret_send, ret_recv.at[block, k], to_z, i, tp).start()
+
+    def answer_plane(k, some):
+        def send_own(j, _):
+            to = (inner + j) % GROUP
+            for at, block in some:
+                answer(k, at, first_group[block] + inner, block, z, to)
+            return 0
+
+        lax.fori_loop(1, GROUP, send_own, 0)
+        for at, block in some:
             returned[k, first_group[block] + inner] = product[k, at * GROUP + inner]
+
+    def answer_near(k):
+        answer_plane(k, ways[2:4])
+        answer_plane(k, ways[4:5])
 
     def weighed(block, groups, k):
         remotes = groups - 1
         landed(returned.at[k, pl.ds(0, remotes)], ret_recv.at[block, k])
-        rows = returned[k, pl.ds(first_group[block], groups)].reshape(groups * CAP, COL)
+        rows = returned[k, pl.ds(first_group[block], groups)].reshape(groups * CAP, HALF)
         lanes = slice(LANE[block], LANE[block] + groups * CAP)
         return jnp.dot(high[:, lanes], rows, preferred_element_type=F32) + jnp.dot(
             low[:, lanes], rows, preferred_element_type=F32
@@ -387,45 +415,69 @@
             remote(near.at[side, k], near_in.at[side, k], near_send, near_recv.at[side, k], to, inner, tp).start()
 
     def close(k):
-        n = columns_at(k)
+        n, h = columns_at(k)
         here = weighed(BLOCK_E, 8, k)
         landed(near_in.at[0, k], near_recv.at[0, k])
         landed(near_in.at[1, k], near_recv.at[1, k])
-        t = tokens[:, pl.ds(pl.multiple_of(n * COL, COL), COL)].astype(F32)
+        t = tokens[:, pl.ds(pl.multiple_of(n * COL + h * HALF, HALF), HALF)].astype(F32)
         r = (t + here + near_in[0, k].astype(F32) + near_in[1, k].astype(F32)).astype(BF16)
         residual[k] = r
         s = r.astype(F32)
         s = s * s
-        s = s[:, 0:128] + s[:, 128:256] + s[:, 256:384] + s[:, 384:512]
+        s = s[:, 0:128] + s[:, 128:256]
         squares[...] = s if k == 0 else squares[...] + s
 
         @pl.when(n != tp)
         def _():
-            remote(residual.at[k], slices.at[tp], slice_send, slice_recv.at[tp], z, inner, n).start()
+            remote(residual.at[k], slices.at[tp, h], slice_send, slice_recv.at[tp], z, inner, n).start()
 
         @pl.when(n == tp)
         def _():
-            slices[tp] = residual[k]
+            slices[tp, h] = residual[k]
 
     contract(0)
+    contract(1)
+    answer_near(0)
     relay_down(1)
-    contract(1)
-    relay_down(2)
+    answer_near(1)
     send_partials(0)
-    relay_down(3)
     contract(2)
     send_partials(1)
+    answer_near(2)
+    relay_down(2)
+    contract(3)
+    answer_near(3)
     add_partials(0)
-    contract(3)
     send_partials(2)
     add_partials(1)
+    relay_down(3)
     close(0)
+    contract(4)
+    answer_near(4)
     send_partials(3)
     add_partials(2)
     close(1)
+    contract(5)
+    answer_near(5)
+    send_partials(4)
     add_partials(3)
     close(2)
+    contract(6)
+    answer_near(6)
+    send_partials(5)
+    add_partials(4)
     close(3)
+    contract(7)
+    answer_near(7)
+    send_partials(6)
+    add_partials(5)
+    close(4)
+    send_partials(7)
+    add_partials(6)
+    close(5)
+    add_partials(7)
+    close(6)
+    close(7)
 
     inverse = lax.rsqrt(jnp.sum(squares[...], axis=-1, keepdims=True) / D + EPS)
     inverse_out[...] = jnp.broadcast_to(inverse, (ROWS, 128)).T[0:8, :]
@@ -438,17 +490,23 @@
 
     def finish(source):
         column = jnp.broadcast_to(inverses[source, 0:1, :], (128, ROWS)).T[:, 0:1]
-        out[source] = (slices[source].astype(F32) * column * final_gain[...].astype(F32)[None, :]).astype(BF16)
+        for h in range(2):
+            cols = slice(h * HALF, (h + 1) * HALF)
+            t = slices[source, h].astype(F32) * column * final_gain[cols].astype(F32)[None, :]
+            done[source, :, cols] = t.astype(BF16)
 
     finish(tp)
-    for copy in lasts:
+    for copy, other in zip(lasts, (left, right, opposite)):
         copy.wait_recv()
-    for other in (right, left, opposite):
         landed(slices.at[other], slice_recv.at[other])
         finish(other)
+    results = [pltpu.make_async_copy(done.at[n], out.at[n], done_sem.at[n]) for n in range(TP)]
+    start(results)
 
     for copy in tells + flights + lasts + sum(outs, []) + sum(ons, []):
         copy.wait_send()
+    for copy in results:
+        copy.wait()
     sent(raw, raw_send)
     sent(routed.at[pl.ds(0, 59)], disp_send)
     sent(routed.at[pl.ds(0, 59)], ret_send)
@@ -460,15 +518,21 @@
 def local(
     tokens, norm_gain, expert_ids, group_weight, expert_logit, w_gate, w_up, w_down, final_gain
 ):
-    vmem = pl.BlockSpec(memory_space=pltpu.VMEM)
     anywhere = pl.BlockSpec(memory_space=pl.ANY)
     dma, groups = pltpu.SemaphoreType.DMA, PLANES * GROUP
     out = pl.pallas_call(
         kernel,
         out_shape=jax.ShapeDtypeStruct((TP, ROWS, COL), BF16),
-        in_specs=[vmem] * 5 + [anywhere] * 3 + [vmem],
-        out_specs=vmem,
+        in_specs=[anywhere] * 9,
+        out_specs=anywhere,
         scratch_shapes=[
+            pltpu.VMEM((ROWS, D), BF16),
+            pltpu.VMEM((D,), BF16),
+            pltpu.VMEM((2, ROWS), jnp.int32),
+            pltpu.VMEM((1, ROWS), F32),
+            pltpu.VMEM((2, ROWS), F32),
+            pltpu.VMEM((COL,), BF16),
+            pltpu.VMEM((TP, ROWS, COL), BF16),
             pltpu.VMEM((TP, ROWS, COL), BF16),
             pltpu.VMEM((4, TP, ROWS, COL), BF16),
             pltpu.VMEM((5, 8, ROWS), F32),
@@ -476,24 +540,24 @@
             pltpu.VMEM((groups, CAP, D), BF16),
             pltpu.VMEM((groups, CAP, D), BF16),
             pltpu.VMEM((TP, groups * CAP, FF // TP), BF16),
-            pltpu.VMEM((TP, groups, CAP, COL), BF16),
-            pltpu.VMEM((TP, groups, CAP, COL), BF16),
+            pltpu.VMEM((STAGES, groups, CAP, HALF), BF16),
+            pltpu.VMEM((STAGES, groups, CAP, HALF), BF16),
             pltpu.VMEM((TP, D, FF // TP), BF16),
             pltpu.VMEM((TP, D, FF // TP), BF16),
             pltpu.VMEM((TP, TP, FF // TP, COL), BF16),
             pltpu.VMEM((ROWS, 1152), BF16),
             pltpu.VMEM((ROWS, 1152), BF16),
-            pltpu.VMEM((2, TP, ROWS, COL), BF16),
-            pltpu.VMEM((2, TP, ROWS, COL), BF16),
-            pltpu.VMEM((2, TP, ROWS, COL), BF16),
-            pltpu.VMEM((2, TP, ROWS, COL), BF16),
-            pltpu.VMEM((TP, ROWS, COL), BF16),
-            pltpu.VMEM((TP, ROWS, COL), BF16),
+            pltpu.VMEM((2, STAGES, ROWS, HALF), BF16),
+            pltpu.VMEM((2, STAGES, ROWS, HALF), BF16),
+            pltpu.VMEM((2, STAGES, ROWS, HALF), BF16),
+            pltpu.VMEM((2, STAGES, ROWS, HALF), BF16),
+            pltpu.VMEM((STAGES, ROWS, HALF), BF16),
+            pltpu.VMEM((TP, 2, ROWS, HALF), BF16),
             pltpu.VMEM((ROWS, 128), F32),
             pltpu.VMEM((8, ROWS), F32),
             pltpu.VMEM((TP, 8, ROWS), F32),
-            dma((6,)), dma((6,)), dma((6,)), dma((TP, 6)), dma((TP, 6)), dma((4,)), dma((4,)), dma, dma((4, TP)),
-            dma, dma((PLANES,)), dma, dma((5, TP)), dma, dma((2, TP)), dma, dma((2, TP)), dma, dma((TP,)),
+            dma((6,)), dma((TP,)), dma((6,)), dma((6,)), dma((6,)), dma((TP, 6)), dma((TP, 6)), dma((4,)), dma((4,)), dma, dma((4, TP)),
+            dma, dma((PLANES,)), dma, dma((5, STAGES)), dma, dma((2, STAGES)), dma, dma((2, STAGES)), dma, dma((TP,)),
             dma((3,)), dma((3,)),
         ],
         compiler_params=pltpu.CompilerParams(

time: 185 us -> 176 us (0.951)
  the two profiles are of different devices: /device:TPU:8 before, /device:TPU:1 now
where the time goes in v5:
time: 176 us; the launch traced here: 173 us
  Pallas kernels  170 us (97%)
  local copies, waits for them, and re-layouts  2.26 us (1%)
    pallas_call x1, Pallas kernels, local(): pl.pallas_call(kernel, out_shape=jax.ShapeDtypeStruct((TP, ROWS, COL), BF...  170 us

profile of v5, /device:TPU:1, one launch (start us, length us, event | category | flops | bytes accessed | tf_op | source)
XLA Modules:
  0.0 172.6 jit_solution(10522899229042174462)
XLA Ops:
  0.0 170.4 %shard_map.91 = bf16[4,256,512]{2,1,0:T(8,128)(2,1)} custom-call(bf16[256,2048]{1,0:T(8,128)(2,1)} %tokens_in.1, bf16[2048]{0:T(1024)(128)(2,1)} %gain_in.1, s32[2,256]{1,0:T(2,128)} %bitcast.11, f32[1,256]{1,0:T(1,128)} %bitcast.13, f32[2,256]{1,0:T(2,128)} %bitcast.12, bf16[2048,256]{1,0:T(8,128)(2,1)} %bitcast.8, bf16[2048,256]{1,0:T(8,128)(2,1)} %bitcast.9, ...), custom_call_target="tpu_custom_call" | custom-call | tf_op jit(solution)/shard_map/pallas_call | solution.py:523
  170.4 2.3 %copy.11 = bf16[1024,512]{1,0:T(8,128)(2,1)} copy(bf16[1024,512]{1,0:T(8,128)(2,1)} %bitcast.7) | data formatting | bytes 2097152

commit v6 on v5

--- a/solution.py
+++ b/solution.py
@@ -29,10 +29,10 @@
 
 def kernel(
     tokens_in, gain_in, ids_in, group_weight_in, logit_in, w_gate, w_up, w_down, final_gain_in, out,
-    tokens, gain, ids, group_weight, logit, final_gain, done,
+    tokens, gain, ids, group_weight, logit, final_gain,
     normed, raw, info, pick, packed, routed, hidden, product, returned, wg, wu, wd, high, low,
     far, far_in, near, near_in, residual, slices, squares, inverse_out, inverses,
-    in_sem, done_sem, own_sem, w_send, w_recv, d_send, d_recv, info_send, info_recv, raw_send, raw_recv, disp_send, disp_recv,
+    in_sem, own_sem, w_send, w_recv, d_send, d_recv, info_send, info_recv, raw_send, raw_recv, disp_send, disp_recv,
     ret_send, ret_recv, far_send, far_recv, near_send, near_recv, slice_send, slice_recv, inv_send, inv_recv,
 ):
     ep, tp = lax.axis_index("ep"), lax.axis_index("tp")
@@ -233,17 +233,18 @@
     half = FF // TP // 2
     top, bottom = pl.ds(0, half), pl.ds(half, half)
 
-    def over_y(q, n, part, k, to):
-        return remote(wd.at[q, n, part], wd.at[q, n, part], d_send.at[n, k], d_recv.at[n, k], z, inner, to)
-
-    def down_out(n):
+    def over_y(q, piece, part, k, to):
+        block = wd.at[q, piece % TP, part, pl.ds(piece // TP * HALF, HALF)]
+        return remote(block, block, d_send.at[piece, k], d_recv.at[piece, k], z, inner, to)
+
+    def down_out(piece):
         return [
-            over_y(tp, n, top, 0, right), over_y(tp, n, bottom, 1, left),
-            over_y(tp, n, bottom, 4, right), over_y(tp, n, top, 5, left),
+            over_y(tp, piece, top, 0, right), over_y(tp, piece, bottom, 1, left),
+            over_y(tp, piece, bottom, 4, right), over_y(tp, piece, top, 5, left),
         ]
 
-    def down_on(n):
-        return [over_y(left, n, top, 2, right), over_y(right, n, bottom, 3, left)]
+    def down_on(piece):
+        return [over_y(left, piece, top, 2, right), over_y(right, piece, bottom, 3, left)]
 
     def start(copies):
         for copy in copies:
@@ -253,15 +254,15 @@
     flights.append(weights(wg.at[left], wg.at[left], 4, right))
     flights[1].wait_recv()
     flights.append(weights(wu.at[right], wu.at[right], 5, left))
-    outs, ons = [down_out(n) for n in (0, 2, 3, 1)], [down_on(n) for n in (0, 2, 3, 1)]
+    outs, ons = [down_out(k) for k in range(STAGES)], [down_on(k) for k in range(STAGES)]
     start(outs[0])
 
     def relay_down(k):
         outs[k][0].wait_recv()
         outs[k][1].wait_recv()
         start(ons[k])
-        if k + 1 < TP:
-            start(outs[k + 1])
+        for later in ((1,), (2,), (3, 4), (5,), (6,), (7,), (), ())[k]:
+            start(outs[later])
 
     def expand(q, first_row, count):
         groups = count // CAP
@@ -338,24 +339,25 @@
     rows_landed(AT_FAR, GROUP)
     expand_of((0, 1, 4), 640, 384)
 
-    last = tp // 3
-
     def columns_at(k):
-        if k < 5:
-            return (0, 0, 2, 2, 3)[k], k % 2
-        return (3 - 2 * last, 1, 1 + 2 * last)[k - 5], (1 - last, last, 1)[k - 5]
+        if k < TP:
+            return k, 0
+        if k < STAGES - 1:
+            return k - TP + (k - tp) // TP, 1
+        return tp, 1
 
     odd = inner % 2
     ways = ((AT_A, BLOCK_A), (AT_B, BLOCK_B), (AT_C, BLOCK_C), (AT_D, BLOCK_D), (AT_E, BLOCK_E))
 
     def contract(k):
         n, h = columns_at(k)
-        cols = pl.ds(pl.multiple_of(h * HALF, HALF), HALF)
-        if k in (0, 2, 4, 5):
-            for sem in range(2, 6):
-                landed(wd.at[opposite, 0, top], d_recv.at[(0, 0, 2, 2, 3, 1)[k], sem])
+        cols = pl.ds(h * HALF, HALF)
+        for piece in ((0,), (1,), (2,), (3,), (4, 5), (6,), (7,), ())[k]:
+            for copy in outs[piece][2:] + ons[piece]:
+                copy.wait_recv()
 
         def part(i, _):
+            i = 3 - i
             at = pl.ds(pl.multiple_of(i * 256, 256), 256)
             rows = jnp.dot(hidden[0, at, :], wd[0, n, :, cols], preferred_element_type=F32)
             for q in range(1, TP):
@@ -363,7 +365,7 @@
             product[k, pl.ds(i * 16, 16)] = rows.astype(BF16).reshape(16, CAP, HALF)
             return 0
 
-        lax.fori_loop(0, 4, part, 0)
+        lax.fori_loop(0, 2, part, 0)
 
         def send_far(i, _):
             answer(k, AT_FAR, A + 16 + inner // 2 + (B - A) * odd, odd, (z + 6 + 4 * odd) % PLANES, i)
@@ -372,6 +374,7 @@
             return 0
 
         lax.fori_loop(0, GROUP, send_far, 0)
+        lax.fori_loop(2, 4, part, 0)
         answer_plane(k, ways[0:2])
 
     def answer(k, at, group, block, to_z, i):
@@ -435,24 +438,28 @@
         def _():
             slices[tp, h] = residual[k]
 
+    relay_down(1)
     contract(0)
     contract(1)
     answer_near(0)
-    relay_down(1)
+    relay_down(2)
     answer_near(1)
     send_partials(0)
     contract(2)
+    relay_down(3)
     send_partials(1)
     answer_near(2)
-    relay_down(2)
     contract(3)
+    relay_down(4)
     answer_near(3)
     add_partials(0)
     send_partials(2)
+    relay_down(5)
     add_partials(1)
-    relay_down(3)
+    relay_down(6)
     close(0)
     contract(4)
+    relay_down(7)
     answer_near(4)
     send_partials(3)
     add_partials(2)
@@ -493,20 +500,16 @@
         for h in range(2):
             cols = slice(h * HALF, (h + 1) * HALF)
             t = slices[source, h].astype(F32) * column * final_gain[cols].astype(F32)[None, :]
-            done[source, :, cols] = t.astype(BF16)
+            out[source, :, cols] = t.astype(BF16)
 
     finish(tp)
     for copy, other in zip(lasts, (left, right, opposite)):
         copy.wait_recv()
         landed(slices.at[other], slice_recv.at[other])
         finish(other)
-    results = [pltpu.make_async_copy(done.at[n], out.at[n], done_sem.at[n]) for n in range(TP)]
-    start(results)
 
     for copy in tells + flights + lasts + sum(outs, []) + sum(ons, []):
         copy.wait_send()
-    for copy in results:
-        copy.wait()
     sent(raw, raw_send)
     sent(routed.at[pl.ds(0, 59)], disp_send)
     sent(routed.at[pl.ds(0, 59)], ret_send)
@@ -522,9 +525,9 @@
     dma, groups = pltpu.SemaphoreType.DMA, PLANES * GROUP
     out = pl.pallas_call(
         kernel,
-        out_shape=jax.ShapeDtypeStruct((TP, ROWS, COL), BF16),
+        out_shape=pltpu.VMEM((TP, ROWS, COL), BF16),
         in_specs=[anywhere] * 9,
-        out_specs=anywhere,
+        out_specs=pl.BlockSpec(memory_space=pltpu.VMEM),
         scratch_shapes=[
             pltpu.VMEM((ROWS, D), BF16),
             pltpu.VMEM((D,), BF16),
@@ -532,7 +535,6 @@
             pltpu.VMEM((1, ROWS), F32),
             pltpu.VMEM((2, ROWS), F32),
             pltpu.VMEM((COL,), BF16),
-            pltpu.VMEM((TP, ROWS, COL), BF16),
             pltpu.VMEM((TP, ROWS, COL), BF16),
             pltpu.VMEM((4, TP, ROWS, COL), BF16),
             pltpu.VMEM((5, 8, ROWS), F32),
@@ -556,7 +558,7 @@
             pltpu.VMEM((ROWS, 128), F32),
             pltpu.VMEM((8, ROWS), F32),
             pltpu.VMEM((TP, 8, ROWS), F32),
-            dma((6,)), dma((TP,)), dma((6,)), dma((6,)), dma((6,)), dma((TP, 6)), dma((TP, 6)), dma((4,)), dma((4,)), dma, dma((4, TP)),
+            dma((6,)), dma((6,)), dma((6,)), dma((6,)), dma((STAGES, 6)), dma((STAGES, 6)), dma((4,)), dma((4,)), dma, dma((4, TP)),
             dma, dma((PLANES,)), dma, dma((5, STAGES)), dma, dma((2, STAGES)), dma, dma((2, STAGES)), dma, dma((TP,)),
             dma((3,)), dma((3,)),
         ],

time: 176 us -> 167 us (0.949); the launches traced: 173 us -> 167 us
  Pallas kernels: 170 us -> 166 us
    pallas_call x1, Pallas kernels: 170 us -> 166 us  [local(): pl.pallas_call(kernel, out_shape=pltpu.VMEM((TP, ROWS, COL), BF16), in_sp...]
where the time goes in v6:
time: 167 us
  Pallas kernels  166 us (99%)
    pallas_call x1, Pallas kernels, local(): pl.pallas_call(kernel, out_shape=pltpu.VMEM((TP, ROWS, COL), BF16), in_sp...  166 us

profile of v6, /device:TPU:1, one launch (start us, length us, event | category | flops | bytes accessed | tf_op | source)
XLA Modules:
  0.0 166.8 jit_solution(10514700481625851584)
XLA Ops:
  0.0 165.8 %shard_map.91 = bf16[4,256,512]{2,1,0:T(8,128)(2,1)S(1)} custom-call(bf16[256,2048]{1,0:T(8,128)(2,1)} %tokens_in.1, bf16[2048]{0:T(1024)(128)(2,1)} %gain_in.1, s32[2,256]{1,0:T(2,128)} %bitcast.11, f32[1,256]{1,0:T(1,128)} %bitcast.13, f32[2,256]{1,0:T(2,128)} %bitcast.12, bf16[2048,256]{1,0:T(8,128)(2,1)} %bitcast.8, bf16[2048,256]{1,0:T(8,128)(2,1)} %bitcast.9, ...), custom_call_target="tpu_custom_call" | custom-call | tf_op jit(solution)/shard_map/pallas_call | solution.py:526
  165.8 1.0 copy.11

commit v7 on v6

--- a/solution.py
+++ b/solution.py
@@ -30,7 +30,7 @@
 def kernel(
     tokens_in, gain_in, ids_in, group_weight_in, logit_in, w_gate, w_up, w_down, final_gain_in, out,
     tokens, gain, ids, group_weight, logit, final_gain,
-    normed, raw, info, pick, packed, routed, hidden, product, returned, wg, wu, wd, high, low,
+    normed, raw, info, pick, packed, routed, hidden, product, returned, wgu, wd, high, low,
     far, far_in, near, near_in, residual, slices, squares, inverse_out, inverses,
     in_sem, own_sem, w_send, w_recv, d_send, d_recv, info_send, info_recv, raw_send, raw_recv, disp_send, disp_recv,
     ret_send, ret_recv, far_send, far_recv, near_send, near_recv, slice_send, slice_recv, inv_send, inv_recv,
@@ -47,10 +47,10 @@
         )
 
     def landed(dst, recv):
-        remote(dst, dst, info_send.at[0], recv, z, inner, right).wait_recv()
+        remote(dst, dst, info_send, recv, z, inner, right).wait_recv()
 
     def sent(src, send):
-        remote(src, src, send, info_recv.at[0], z, inner, right).wait_send()
+        remote(src, src, send, info_recv, z, inner, right).wait_send()
 
     barrier = pltpu.get_barrier_semaphore()
 
@@ -74,24 +74,26 @@
         greet(z, inner, other)
 
     inputs = [
-        pltpu.make_async_copy(src, dst, in_sem.at[k])
+        pltpu.make_async_copy(tokens_in.at[pl.ds(n * 64, 64)], tokens.at[pl.ds(n * 64, 64)], in_sem.at[n])
+        for n in range(4)
+    ] + [
+        pltpu.make_async_copy(src, dst, in_sem.at[4 + k])
         for k, (src, dst) in enumerate((
-            (tokens_in, tokens), (gain_in, gain), (ids_in, ids), (group_weight_in, group_weight),
-            (logit_in, logit), (final_gain_in, final_gain),
+            (gain_in, gain), (ids_in, ids), (group_weight_in, group_weight), (logit_in, logit),
+            (final_gain_in, final_gain),
         ))
     ]
-    for copy in inputs:
-        copy.start()
+    gate_part, up_part = pl.ds(0, FF // TP), pl.ds(FF // TP, FF // TP)
     own = [
-        pltpu.make_async_copy(w_gate, wg.at[tp], own_sem.at[0]),
-        pltpu.make_async_copy(w_up, wu.at[tp], own_sem.at[1]),
+        pltpu.make_async_copy(w_gate, wgu.at[tp, :, gate_part], own_sem.at[0]),
+        pltpu.make_async_copy(w_up, wgu.at[tp, :, up_part], own_sem.at[1]),
     ] + [
         pltpu.make_async_copy(w_down.at[:, pl.ds(n * COL, COL)], wd.at[tp, n], own_sem.at[2 + n]) for n in range(TP)
     ]
-    for copy in inputs:
+    for copy in inputs + own[:2]:
+        copy.start()
+    for copy in inputs[4:]:
         copy.wait()
-    for copy in own:
-        copy.start()
 
     def norm_rows(i, _):
         at = pl.ds(pl.multiple_of(i * 32, 32), 32)
@@ -102,23 +104,28 @@
             normed[n, at, :] = t[:, n * COL:(n + 1) * COL]
         return 0
 
-    lax.fori_loop(0, ROWS // 32, norm_rows, 0)
-
-    for copy in own:
+    for n in range(4):
+        inputs[n].wait()
+        lax.fori_loop(2 * n, 2 * n + 2, norm_rows, 0)
+
+    for copy in own[:2]:
         copy.wait()
     pl.semaphore_wait(barrier, 42)
 
-    def weights(src, dst, k, to):
-        copy = remote(src, dst, w_send.at[k], w_recv.at[k], z, inner, to)
+    def weights(q, part, k, to):
+        block = wgu.at[q, :, part]
+        copy = remote(block, block, w_send, w_recv.at[k], z, inner, to)
         copy.start()
         return copy
 
     flights = [
-        weights(wg.at[tp], wg.at[tp], 0, right),
-        weights(wu.at[tp], wu.at[tp], 1, left),
-        weights(wu.at[tp], wu.at[tp], 2, right),
-        weights(wg.at[tp], wg.at[tp], 3, left),
+        weights(tp, gate_part, 0, right),
+        weights(tp, up_part, 1, left),
+        weights(tp, up_part, 2, right),
+        weights(tp, gate_part, 3, left),
     ]
+    for copy in own[2:]:
+        copy.start()
 
     id0, id1 = ids[0:1, :], ids[1:2, :]
     lane = lax.broadcasted_iota(jnp.int32, (PLANES * GROUP, ROWS), 0)
@@ -192,7 +199,7 @@
             routed[at * GROUP + inner, :, cols] = packed[first_group[block] + inner, :, cols]
 
     tells = [
-        remote(info.at[BLOCK_E], info.at[block], info_send.at[block], info_recv.at[block], to, inner, tp)
+        remote(info.at[BLOCK_E], info.at[block], info_send, info_recv, to, inner, tp)
         for block, to in ((BLOCK_C, up1), (BLOCK_D, down1), (BLOCK_A, up2), (BLOCK_B, down2))
     ]
     for copy in tells:
@@ -200,7 +207,7 @@
 
     def hop_out(n, _):
         remote(normed.at[n], raw.at[0, n], raw_send, raw_recv.at[0, n], up1, inner, tp).start()
-        remote(normed.at[n], raw.at[1, n], raw_send, raw_recv.at[1, n], down1, inner, tp).start()
+        remote(normed.at[n], raw.at[1, n], raw_send, raw_recv.at[0, n], down1, inner, tp).start()
         return 0
 
     lax.fori_loop(0, TP, hop_out, 0)
@@ -213,16 +220,14 @@
         return 0
 
     lax.fori_loop(0, TP, pack_own, 0)
-    for copy in tells:
-        copy.wait_recv()
+    landed(info.at[pl.ds(0, 4)], info_recv)
     for block in (BLOCK_C, BLOCK_D, BLOCK_A, BLOCK_B):
         make_pick(block)
 
     def hop_on(n, _):
-        landed(raw.at[0, n], raw_recv.at[0, n])
-        remote(raw.at[0, n], raw.at[2, n], raw_send, raw_recv.at[2, n], up1, inner, tp).start()
-        landed(raw.at[1, n], raw_recv.at[1, n])
-        remote(raw.at[1, n], raw.at[3, n], raw_send, raw_recv.at[3, n], down1, inner, tp).start()
+        landed(raw.at[0, pl.ds(0, 2)], raw_recv.at[0, n])
+        remote(raw.at[0, n], raw.at[2, n], raw_send, raw_recv.at[1, n], up1, inner, tp).start()
+        remote(raw.at[1, n], raw.at[3, n], raw_send, raw_recv.at[1, n], down1, inner, tp).start()
         pack(BLOCK_C, 8, raw[0, n], n)
         pack(BLOCK_D, 8, raw[1, n], n)
         send_own_plane(((BLOCK_C, AT_C), (BLOCK_D, AT_D)), n)
@@ -235,31 +240,32 @@
 
     def over_y(q, piece, part, k, to):
         block = wd.at[q, piece % TP, part, pl.ds(piece // TP * HALF, HALF)]
-        return remote(block, block, d_send.at[piece, k], d_recv.at[piece, k], z, inner, to)
+        return remote(block, block, d_send, d_recv.at[piece, k], z, inner, to)
 
     def down_out(piece):
         return [
-            over_y(tp, piece, top, 0, right), over_y(tp, piece, bottom, 1, left),
-            over_y(tp, piece, bottom, 4, right), over_y(tp, piece, top, 5, left),
+            over_y(tp, piece, top, 0, right), over_y(tp, piece, bottom, 0, left),
+            over_y(tp, piece, bottom, 1, right), over_y(tp, piece, top, 1, left),
         ]
 
     def down_on(piece):
-        return [over_y(left, piece, top, 2, right), over_y(right, piece, bottom, 3, left)]
+        return [over_y(left, piece, top, 1, right), over_y(right, piece, bottom, 1, left)]
 
     def start(copies):
         for copy in copies:
             copy.start()
 
     flights[0].wait_recv()
-    flights.append(weights(wg.at[left], wg.at[left], 4, right))
+    flights.append(weights(left, gate_part, 4, right))
     flights[1].wait_recv()
-    flights.append(weights(wu.at[right], wu.at[right], 5, left))
+    flights.append(weights(right, up_part, 5, left))
     outs, ons = [down_out(k) for k in range(STAGES)], [down_on(k) for k in range(STAGES)]
+    for copy in own[2:]:
+        copy.wait()
     start(outs[0])
 
     def relay_down(k):
-        outs[k][0].wait_recv()
-        outs[k][1].wait_recv()
+        landed(wd.at[0, 0, :, pl.ds(0, HALF)], d_recv.at[k, 0])
         start(ons[k])
         for later in ((1,), (2,), (3, 4), (5,), (6,), (7,), (), ())[k]:
             start(outs[later])
@@ -267,8 +273,8 @@
     def expand(q, first_row, count):
         groups = count // CAP
         xs = routed[pl.ds(first_row // CAP, groups)].reshape(count, D)
-        g = jnp.dot(xs, wg[q], preferred_element_type=F32)
-        u = jnp.dot(xs, wu[q], preferred_element_type=F32)
+        both = jnp.dot(xs, wgu[q], preferred_element_type=F32)
+        g, u = both[:, :FF // TP], both[:, FF // TP:]
         hidden[q, pl.ds(first_row, count), :] = (g / (1.0 + jnp.exp(-g)) * u).astype(BF16)
 
     def expand_of(order, first_row, count):
@@ -289,8 +295,7 @@
     expand_of((0, 0, 1), 0, 384)
 
     def hop_last(n, _):
-        landed(raw.at[2, n], raw_recv.at[2, n])
-        landed(raw.at[3, n], raw_recv.at[3, n])
+        landed(raw.at[0, pl.ds(0, 2)], raw_recv.at[1, n])
         pack(BLOCK_A, 20, raw[2, n], n)
         pack(BLOCK_B, 20, raw[3, n], n)
         send_own_plane(((BLOCK_A, AT_A), (BLOCK_B, AT_B)), n)
@@ -353,8 +358,7 @@
         n, h = columns_at(k)
         cols = pl.ds(h * HALF, HALF)
         for piece in ((0,), (1,), (2,), (3,), (4, 5), (6,), (7,), ())[k]:
-            for copy in outs[piece][2:] + ons[piece]:
-                copy.wait_recv()
+            landed(wd.at[0, 0], d_recv.at[piece, 1])
 
         def part(i, _):
             i = 3 - i
@@ -368,7 +372,7 @@
         lax.fori_loop(0, 2, part, 0)
 
         def send_far(i, _):
-            answer(k, AT_FAR, A + 16 + inner // 2 + (B - A) * odd, odd, (z + 6 + 4 * odd) % PLANES, i)
+            answer(k, AT_FAR, A + 16 + inner // 2 + (B - A) * odd, BLOCK_A, (z + 6 + 4 * odd) % PLANES, i)
             answer(k, AT_UP, A + 8 + inner, BLOCK_A, down1, i)
             answer(k, AT_DOWN, B + 8 + inner, BLOCK_B, up1, i)
             return 0
@@ -378,7 +382,7 @@
         answer_plane(k, ways[0:2])
 
     def answer(k, at, group, block, to_z, i):
-        remote(product.at[k, at * GROUP + i], returned.at[k, group], ret_send, ret_recv.at[block, k], to_z, i, tp).start()
+        remote(product.at[k, at * GROUP + i], returned.at[k, group], ret_send, ret_recv.at[block // 2, k], to_z, i, tp).start()
 
     def answer_plane(k, some):
         def send_own(j, _):
@@ -396,8 +400,6 @@
         answer_plane(k, ways[4:5])
 
     def weighed(block, groups, k):
-        remotes = groups - 1
-        landed(returned.at[k, pl.ds(0, remotes)], ret_recv.at[block, k])
         rows = returned[k, pl.ds(first_group[block], groups)].reshape(groups * CAP, HALF)
         lanes = slice(LANE[block], LANE[block] + groups * CAP)
         return jnp.dot(high[:, lanes], rows, preferred_element_type=F32) + jnp.dot(
@@ -405,23 +407,25 @@
         )
 
     def send_partials(k):
+        landed(returned.at[k, pl.ds(0, 38)], ret_recv.at[0, k])
         far[0, k] = weighed(BLOCK_A, 20, k).astype(BF16)
-        remote(far.at[0, k], far_in.at[0, k], far_send, far_recv.at[0, k], down1, inner, tp).start()
+        remote(far.at[0, k], far_in.at[0, k], far_send, far_recv.at[k], down1, inner, tp).start()
         far[1, k] = weighed(BLOCK_B, 20, k).astype(BF16)
-        remote(far.at[1, k], far_in.at[1, k], far_send, far_recv.at[1, k], up1, inner, tp).start()
+        remote(far.at[1, k], far_in.at[1, k], far_send, far_recv.at[k], up1, inner, tp).start()
 
     def add_partials(k):
+        landed(returned.at[k, pl.ds(0, 14)], ret_recv.at[1, k])
+        landed(far_in.at[0, pl.ds(0, 2)], far_recv.at[k])
         for side, block, to in ((0, BLOCK_C, down1), (1, BLOCK_D, up1)):
             here = weighed(block, 8, k)
-            landed(far_in.at[side, k], far_recv.at[side, k])
             near[side, k] = (here + far_in[side, k].astype(F32)).astype(BF16)
-            remote(near.at[side, k], near_in.at[side, k], near_send, near_recv.at[side, k], to, inner, tp).start()
+            remote(near.at[side, k], near_in.at[side, k], near_send, near_recv.at[k], to, inner, tp).start()
 
     def close(k):
         n, h = columns_at(k)
+        landed(returned.at[k, pl.ds(0, 7)], ret_recv.at[2, k])
         here = weighed(BLOCK_E, 8, k)
-        landed(near_in.at[0, k], near_recv.at[0, k])
-        landed(near_in.at[1, k], near_recv.at[1, k])
+        landed(near_in.at[0, pl.ds(0, 2)], near_recv.at[k])
         t = tokens[:, pl.ds(pl.multiple_of(n * COL + h * HALF, HALF), HALF)].astype(F32)
         r = (t + here + near_in[0, k].astype(F32) + near_in[1, k].astype(F32)).astype(BF16)
         residual[k] = r
@@ -489,7 +493,7 @@
     inverse = lax.rsqrt(jnp.sum(squares[...], axis=-1, keepdims=True) / D + EPS)
     inverse_out[...] = jnp.broadcast_to(inverse, (ROWS, 128)).T[0:8, :]
     lasts = [
-        remote(inverse_out, inverses.at[tp], inv_send.at[k], inv_recv.at[k], z, inner, other)
+        remote(inverse_out, inverses.at[tp], inv_send, inv_recv.at[k], z, inner, other)
         for k, other in enumerate((right, left, opposite))
     ]
     start(lasts)
@@ -508,8 +512,10 @@
         landed(slices.at[other], slice_recv.at[other])
         finish(other)
 
-    for copy in tells + flights + lasts + sum(outs, []) + sum(ons, []):
-        copy.wait_send()
+    sent(info.at[pl.ds(0, 4)], info_send)
+    sent(wgu.at[pl.ds(0, 3)], w_send)
+    sent(wd.at[pl.ds(0, 3)], d_send)
+    sent(inverses.at[pl.ds(0, 3)], inv_send)
     sent(raw, raw_send)
     sent(routed.at[pl.ds(0, 59)], disp_send)
     sent(routed.at[pl.ds(0, 59)], ret_send)
@@ -544,8 +550,7 @@
             pltpu.VMEM((TP, groups * CAP, FF // TP), BF16),
             pltpu.VMEM((STAGES, groups, CAP, HALF), BF16),
             pltpu.VMEM((STAGES, groups, CAP, HALF), BF16),
-            pltpu.VMEM((TP, D, FF // TP), BF16),
-            pltpu.VMEM((TP, D, FF // TP), BF16),
+            pltpu.VMEM((TP, D, 2 * FF // TP), BF16),
             pltpu.VMEM((TP, TP, FF // TP, COL), BF16),
             pltpu.VMEM((ROWS, 1152), BF16),
             pltpu.VMEM((ROWS, 1152), BF16),
@@ -558,9 +563,9 @@
             pltpu.VMEM((ROWS, 128), F32),
             pltpu.VMEM((8, ROWS), F32),
             pltpu.VMEM((TP, 8, ROWS), F32),
-            dma((6,)), dma((6,)), dma((6,)), dma((6,)), dma((STAGES, 6)), dma((STAGES, 6)), dma((4,)), dma((4,)), dma, dma((4, TP)),
-            dma, dma((PLANES,)), dma, dma((5, STAGES)), dma, dma((2, STAGES)), dma, dma((2, STAGES)), dma, dma((TP,)),
-            dma((3,)), dma((3,)),
+            dma((9,)), dma((6,)), dma, dma((6,)), dma, dma((STAGES, 2)), dma, dma, dma, dma((2, TP)),
+            dma, dma((PLANES,)), dma, dma((3, STAGES)), dma, dma((STAGES,)), dma, dma((STAGES,)), dma, dma((TP,)),
+            dma, dma((3,)),
         ],
         compiler_params=pltpu.CompilerParams(
             collective_id=0, has_side_effects=True, vmem_limit_bytes=62 * 1024 * 1024

time: 167 us -> 166 us (level)
  no operation moved by 1% of the time
where the time goes in v7:
time: 166 us
  Pallas kernels  165 us (99%)
    pallas_call x1, Pallas kernels, local(): pl.pallas_call(kernel, out_shape=pltpu.VMEM((TP, ROWS, COL), BF16), in_sp...  165 us

profile of v7, /device:TPU:1, one launch (start us, length us, event | category | flops | bytes accessed | tf_op | source)
XLA Modules:
  0.0 166.1 jit_solution(1410620163268975811)
XLA Ops:
  0.0 165.1 %shard_map.91 = bf16[4,256,512]{2,1,0:T(8,128)(2,1)S(1)} custom-call(bf16[256,2048]{1,0:T(8,128)(2,1)} %tokens_in.1, bf16[2048]{0:T(1024)(128)(2,1)} %gain_in.1, s32[2,256]{1,0:T(2,128)} %bitcast.11, f32[1,256]{1,0:T(1,128)} %bitcast.13, f32[2,256]{1,0:T(2,128)} %bitcast.12, bf16[2048,256]{1,0:T(8,128)(2,1)} %bitcast.8, bf16[2048,256]{1,0:T(8,128)(2,1)} %bitcast.9, ...), custom_call_target="tpu_custom_call" | custom-call | tf_op jit(solution)/shard_map/pallas_call | solution.py:532
  165.1 1.0 copy.11

commit v8 on v7

--- a/solution.py
+++ b/solution.py
@@ -50,7 +50,11 @@
         remote(dst, dst, info_send, recv, z, inner, right).wait_recv()
 
     def sent(src, send):
-        remote(src, src, send, info_recv, z, inner, right).wait_send()
+        remote(src, src, send, info_recv.at[0], z, inner, right).wait_send()
+
+    def start(copies):
+        for copy in copies:
+            copy.start()
 
     barrier = pltpu.get_barrier_semaphore()
 
@@ -59,18 +63,14 @@
             barrier, inc=1, device_id={"ep": to_z * GROUP + to_inner, "tp": to_tp}, device_id_type=MESH
         )
 
-    def greet_plane(i, _):
-        o = i // GROUP
-        greet((z + PLANES + (1 - 2 * (o % 2)) * (2 - o // 2)) % PLANES, i % GROUP, tp)
-        return 0
-
     def greet_own(j, _):
         greet(z, (inner + j) % GROUP, tp)
         return 0
 
-    lax.fori_loop(0, 4 * GROUP, greet_plane, 0)
+    greet(up1, inner, tp)
+    greet(down1, inner, tp)
     lax.fori_loop(1, GROUP, greet_own, 0)
-    for other in (right, left, opposite):
+    for other in (opposite, right, left):
         greet(z, inner, other)
 
     inputs = [
@@ -110,7 +110,7 @@
 
     for copy in own[:2]:
         copy.wait()
-    pl.semaphore_wait(barrier, 42)
+    pl.semaphore_wait(barrier, 12)
 
     def weights(q, part, k, to):
         block = wgu.at[q, :, part]
@@ -198,12 +198,10 @@
         for block, at in ways:
             routed[at * GROUP + inner, :, cols] = packed[first_group[block] + inner, :, cols]
 
-    tells = [
-        remote(info.at[BLOCK_E], info.at[block], info_send, info_recv, to, inner, tp)
-        for block, to in ((BLOCK_C, up1), (BLOCK_D, down1), (BLOCK_A, up2), (BLOCK_B, down2))
-    ]
-    for copy in tells:
-        copy.start()
+    def tell(block, to, at, k):
+        return remote(info.at[block], info.at[at], info_send, info_recv.at[k], to, inner, tp)
+
+    start([tell(BLOCK_E, up1, BLOCK_C, 0), tell(BLOCK_E, down1, BLOCK_D, 0)])
 
     def hop_out(n, _):
         remote(normed.at[n], raw.at[0, n], raw_send, raw_recv.at[0, n], up1, inner, tp).start()
@@ -220,8 +218,9 @@
         return 0
 
     lax.fori_loop(0, TP, pack_own, 0)
-    landed(info.at[pl.ds(0, 4)], info_recv)
-    for block in (BLOCK_C, BLOCK_D, BLOCK_A, BLOCK_B):
+    landed(info.at[pl.ds(0, 2)], info_recv.at[0])
+    start([tell(BLOCK_C, up1, BLOCK_A, 1), tell(BLOCK_D, down1, BLOCK_B, 1)])
+    for block in (BLOCK_C, BLOCK_D):
         make_pick(block)
 
     def hop_on(n, _):
@@ -251,10 +250,6 @@
     def down_on(piece):
         return [over_y(left, piece, top, 1, right), over_y(right, piece, bottom, 1, left)]
 
-    def start(copies):
-        for copy in copies:
-            copy.start()
-
     flights[0].wait_recv()
     flights.append(weights(left, gate_part, 4, right))
     flights[1].wait_recv()
@@ -287,6 +282,9 @@
     def rows_landed(at, groups):
         landed(routed.at[pl.ds(0, groups)], disp_recv.at[at])
 
+    landed(info.at[pl.ds(0, 2)], info_recv.at[1])
+    for block in (BLOCK_A, BLOCK_B):
+        make_pick(block)
     for block in range(5):
         make_weights(block)
     rows_landed(AT_E, GROUP - 1)
@@ -563,7 +561,7 @@
             pltpu.VMEM((ROWS, 128), F32),
             pltpu.VMEM((8, ROWS), F32),
             pltpu.VMEM((TP, 8, ROWS), F32),
-            dma((9,)), dma((6,)), dma, dma((6,)), dma, dma((STAGES, 2)), dma, dma, dma, dma((2, TP)),
+            dma((9,)), dma((6,)), dma, dma((6,)), dma, dma((STAGES, 2)), dma, dma((2,)), dma, dma((2, TP)),
             dma, dma((PLANES,)), dma, dma((3, STAGES)), dma, dma((STAGES,)), dma, dma((STAGES,)), dma, dma((TP,)),
             dma, dma((3,)),
         ],

time: 166 us -> 165 us (level)
  no operation moved by 1% of the time
where the time goes in v8:
time: 165 us
  Pallas kernels  164 us (99%)
    pallas_call x1, Pallas kernels, local(): pl.pallas_call(kernel, out_shape=pltpu.VMEM((TP, ROWS, COL), BF16), in_sp...  164 us

profile of v8, /device:TPU:1, one launch (start us, length us, event | category | flops | bytes accessed | tf_op | source)
XLA Modules:
  0.0 165.4 jit_solution(897905368409724157)
XLA Ops:
  0.0 164.4 %shard_map.91 = bf16[4,256,512]{2,1,0:T(8,128)(2,1)S(1)} custom-call(bf16[256,2048]{1,0:T(8,128)(2,1)} %tokens_in.1, bf16[2048]{0:T(1024)(128)(2,1)} %gain_in.1, s32[2,256]{1,0:T(2,128)} %bitcast.11, f32[1,256]{1,0:T(1,128)} %bitcast.13, f32[2,256]{1,0:T(2,128)} %bitcast.12, bf16[2048,256]{1,0:T(8,128)(2,1)} %bitcast.8, bf16[2048,256]{1,0:T(8,128)(2,1)} %bitcast.9, ...), custom_call_target="tpu_custom_call" | custom-call | tf_op jit(solution)/shard_map/pallas_call | solution.py:530
  164.4 1.0 copy.11
